TPU v7x, 32 devices: a whole 2x2x4 slice. The times are simulated.
32 devices in a mesh: sp: 4 (over y, x), tp: 8 (over z, core).
Axes of the slice: x: 2, y: 2, z: 4, core: 2. Of those that a mesh axis runs over, the one named last changes fastest.
Arguments:
- moe_input: bfloat16 [1024, 4096], P('sp', 'tp'), may hold values from -6 to 6
- out_gate: bfloat16 [1024, 4096], P('sp', 'tp'), may hold values from -6 to 6
- in_gate: bfloat16 [1024, 4096], P('sp', 'tp'), may hold values from -6 to 6
- values: bfloat16 [1024, 4096], P('sp', 'tp'), may hold values from -6 to 6
- conv_taps: float32 [3, 4096], P(None, 'tp'), may hold values from -3 to 3
- out_proj: bfloat16 [4096, 4096], P(None, 'tp'), may hold values from -0.09375 to 0.09375
- route_ids: int32 [1024, 2], P('sp'), may hold values from 0 to 3, all different within a row; in each aligned block of 256 rows (0 to 255, 256 to 511, ...) at most 192 rows name the same one
- route_gates: float32 [1024, 2], P('sp'), may hold values from 0.1 to 0.9
- expert_gate: bfloat16 [4, 4096, 2048], P('sp', None, 'tp'), may hold values from -0.09375 to 0.09375
- expert_up: bfloat16 [4, 4096, 2048], P('sp', None, 'tp'), may hold values from -0.09375 to 0.09375
- expert_down: bfloat16 [4, 2048, 4096], P('sp', 'tp'), may hold values from -0.125 to 0.125
- cotangent: bfloat16 [1024, 4096], P('sp', 'tp'), may hold values from -6 to 6
Outputs:
- grad_out_gate: bfloat16 [1024, 4096], P('sp', 'tp')
- grad_in_gate: bfloat16 [1024, 4096], P('sp', 'tp')
- grad_values: bfloat16 [1024, 4096], P('sp', 'tp')
- grad_out_proj: float32 [4096, 4096], P('sp', 'tp')
- grad_expert_gate: float32 [4, 4096, 2048], P('sp', None, 'tp')
- grad_expert_up: float32 [4, 4096, 2048], P('sp', None, 'tp')
- grad_expert_down: float32 [4, 2048, 4096], P('sp', 'tp')
Inputs may be any that keep to these rules, and one draw needn't show every extreme that they name: `route_ids`: the 2 experts of a token differ. In the rows of one device no expert is named by more than 192 assignments, and in some device's rows some expert is named by exactly 192.
All inputs are finite; a program needn't handle non-finite values.
Results may differ from a plain program's by a relative error of at most 0.014.
Values may be sent and summed in bfloat16 or wider, within the bound.
A program may use at most 128 MiB of HBM per device.

v0:
```python
import jax
import jax.numpy as jnp
from jax import lax
from jax.experimental import pallas as pl
from jax.experimental.pallas import tpu as pltpu
from jax.sharding import PartitionSpec as P

MESH = pl.DeviceIdType.MESH


def peers_of(group):
    sp, tp = (lax.axis_index("sp"), lax.axis_index("tp"))
    if group == "core":
        me, size = (lax.rem(tp, 2), 2)
    elif group == "z":
        me, size = (lax.div(tp, 2), lax.axis_size("tp") // 2)
    else:
        me, size = (sp, lax.axis_size("sp"))
    others = []
    for k in range(1, size):
        place = lax.rem(me + k, size)
        if group == "core":
            others.append((place, (sp, tp - me + place)))
        elif group == "z":
            others.append((place, (sp, place * 2 + lax.rem(tp, 2))))
        else:
            others.append((place, (place, tp)))
    return me, others


def group_size(group):
    if group == "core":
        return 2
    return lax.axis_size("tp") // 2 if group == "z" else lax.axis_size("sp")


def block(ref, place, width):
    return ref.at[:, pl.ds(pl.multiple_of(place * width, width), width)]


def exchange(collective_id, *ops):
    arrays = [op[2] for op in ops]
    shapes = []
    counts = []
    for kind, group, array, *rest in ops:
        size = group_size(group)
        if kind == "cores":
            shape, count = ((array.shape[0], array.shape[1] // 2), array.shape[1] // rest[0] // 2)
        elif kind == "columns":
            shape = (size - 1, array.shape[0], array.shape[1] // size)
            count = size - 1
        elif kind == "rows":
            shape, count = ((size - 1,) + array.shape[1:], size - 1)
        elif kind == "gather":
            shape, count = ((array.shape[0], array.shape[1] * size), size - 1)
        elif kind == "send":
            shape, count = (array.shape, size - 1)
        elif kind == "stack":
            shape, count = ((size,) + array.shape, size - 1)
        else:
            shape, count = (array.shape, 1)
        shapes.append(jax.ShapeDtypeStruct(shape, array.dtype))
        counts.append(count)
    total = sum(counts)

    def kernel(*refs):
        n = len(ops)
        sources, targets = (refs[:n], refs[n : 2 * n])
        send_sem, recv_sem, own_sem = refs[2 * n :]
        barrier = pltpu.get_barrier_semaphore()
        greeted = 0
        for group in sorted({op[1] for op in ops}):
            for _, device in peers_of(group)[1]:
                pl.semaphore_signal(barrier, inc=1, device_id=device, device_id_type=MESH)
                greeted += 1
        pl.semaphore_wait(barrier, greeted)
        copies = []
        local = []
        for i, (kind, group, array, *rest) in enumerate(ops):
            me, others = peers_of(group)
            source, target = (sources[i], targets[i])
            moves = []
            if kind == "cores":
                width = rest[0]
                place, device = others[0]
                for b in range(counts[i]):
                    moves.append(
                        (
                            block(source, 2 * b + place, width),
                            target.at[:, pl.ds(b * width, width)],
                            device,
                        )
                    )
            for k, (place, device) in enumerate(others):
                if kind == "columns":
                    moves.append((block(source, place, shapes[i].shape[2]), target.at[k], device))
                elif kind == "rows":
                    moves.append((source.at[place], target.at[k], device))
                elif kind == "gather":
                    moves.append((source, block(target, me, array.shape[1]), device))
                elif kind == "send":
                    moves.append((source.at[place], target.at[me], device))
                elif kind == "stack":
                    moves.append((source, target.at[me], device))
                elif kind == "swap":
                    moves.append((source, target, device))
            for a, b, device in moves:
                j = len(copies)
                copy = pltpu.make_async_remote_copy(
                    src_ref=a,
                    dst_ref=b,
                    send_sem=send_sem.at[j],
                    recv_sem=recv_sem.at[j],
                    device_id=device,
                    device_id_type=MESH,
                )
                copy.start()
                copies.append(copy)
            if kind == "gather":
                local.append((source, block(target, me, array.shape[1]), i))
            elif kind == "send":
                local.append((source.at[me], target.at[me], i))
            elif kind == "stack":
                local.append((source, target.at[me], i))
        own = [pltpu.make_async_copy(a, b, own_sem.at[i]) for a, b, i in local]
        for copy in own:
            copy.start()
        for copy in own + copies:
            copy.wait()

    return pl.pallas_call(
        kernel,
        out_shape=shapes,
        in_specs=[pl.BlockSpec(memory_space=pl.ANY)] * len(ops),
        out_specs=[pl.BlockSpec(memory_space=pl.ANY)] * len(ops),
        scratch_shapes=[
            pltpu.SemaphoreType.DMA((total,)),
            pltpu.SemaphoreType.DMA((total,)),
            pltpu.SemaphoreType.DMA((len(ops),)),
        ],
        compiler_params=pltpu.CompilerParams(collective_id=collective_id, has_side_effects=True),
    )(*arrays)


def halves(array, width):
    core = lax.rem(lax.axis_index("tp"), 2)
    blocks = [
        lax.dynamic_slice_in_dim(array, (start + core) * width, width, axis=1)
        for start in range(0, array.shape[1] // width, 2)
    ]
    return jnp.concatenate(blocks, axis=1)


def interleave(own, other, width):
    core = lax.rem(lax.axis_index("tp"), 2)
    first, second = (jnp.where(core == 0, own, other), jnp.where(core == 0, other, own))
    blocks = []
    for start in range(0, own.shape[1], width):
        blocks.append(first[:, start : start + width])
        blocks.append(second[:, start : start + width])
    return jnp.concatenate(blocks, axis=1)


def padded(array, sides, width):
    for axis, dim in sides:
        size, length = (lax.axis_size(axis), array.shape[dim])
        up = [(i, (i + 1) % size) for i in range(size - 1)]
        down = [(j, i) for i, j in up]
        last = lax.slice_in_dim(array, length - width, length, axis=dim)
        initial = lax.slice_in_dim(array, 0, width, axis=dim)
        before = lax.ppermute(last, axis, up)
        after = lax.ppermute(initial, axis, down)
        array = jnp.concatenate([before, array, after], axis=dim)
    return array


def body(
    moe_input,
    out_gate,
    in_gate,
    values,
    conv_taps,
    out_proj,
    route_ids,
    route_gates,
    expert_gate,
    expert_up,
    expert_down,
    cotangent,
):
    token_count = moe_input.shape[0]
    part_width = moe_input.shape[1]
    pick_count = route_ids.shape[1]
    group_count = lax.axis_size("sp")
    local_count = expert_gate.shape[0]
    expert_count = group_count * local_count
    capacity = 3 * token_count // expert_count
    contract_rows = (((0,), (0,)), ((), ()))
    flat_ids = route_ids.reshape(-1)
    one_hot = (flat_ids[:, None] == jnp.arange(expert_count, dtype=jnp.int32)[None, :]).astype(
        jnp.int32
    )
    earlier = jnp.cumsum(one_hot, axis=0) - one_hot
    position = jnp.sum(earlier * one_hot, axis=1)
    slot_index = flat_ids * capacity + position
    block_rows = local_count * capacity
    slots = jnp.arange(expert_count * capacity, dtype=jnp.int32)
    hits = slots[:, None, None] == slot_index.reshape(token_count, pick_count)[None, :, :]
    take = jnp.any(hits, axis=2).astype(jnp.bfloat16)
    slot_weight = jnp.sum(jnp.where(hits, route_gates[None, :, :], 0.0), axis=(1, 2))
    conv_in = in_gate.astype(jnp.float32) * values.astype(jnp.float32)
    rimmed = padded(conv_in, (("sp", 0),), 1)
    conv_out = rimmed[:-2] * conv_taps[0] + rimmed[1:-1] * conv_taps[1] + rimmed[2:] * conv_taps[2]
    mixed = (out_gate.astype(jnp.float32) * conv_out).astype(jnp.bfloat16)
    rows_z, mixed_all = exchange(4, ("gather", "z", moe_input), ("stack", "sp", mixed))
    half = rows_z.shape[1]
    send_rows = jnp.dot(take, rows_z, preferred_element_type=jnp.float32).astype(jnp.bfloat16)
    cot_z, recv_rows = exchange(
        5,
        ("gather", "z", cotangent),
        ("send", "sp", send_rows.reshape(group_count, block_rows, half)),
    )
    send_cot = (
        slot_weight[:, None] * jnp.dot(take, cot_z, preferred_element_type=jnp.float32)
    ).astype(jnp.bfloat16)
    recv_rows = recv_rows.reshape(group_count * block_rows, half)
    recv_cot, swap_rows = exchange(
        6,
        ("send", "sp", send_cot.reshape(group_count, block_rows, half)),
        ("swap", "core", recv_rows),
    )
    recv_cot = recv_cot.reshape(group_count * block_rows, half)
    (swap_cot,) = exchange(7, ("swap", "core", recv_cot))

    def by_expert(own, other):
        full = interleave(own, other, part_width)
        full = full.reshape(group_count, local_count, capacity, 2 * half)
        return jnp.swapaxes(full, 0, 1).reshape(local_count, group_count * capacity, 2 * half)

    full_rows = by_expert(recv_rows, swap_rows)
    full_cot = by_expert(recv_cot, swap_cot)
    pre_gate = jnp.einsum(
        "prd,pdf->prf", full_rows, expert_gate, preferred_element_type=jnp.float32
    )
    pre_up = jnp.einsum("prd,pdf->prf", full_rows, expert_up, preferred_element_type=jnp.float32)
    gate_sig = jax.nn.sigmoid(pre_gate)
    activated = pre_gate * gate_sig
    hidden_act = (activated * pre_up).astype(jnp.bfloat16)
    grad_expert_down = jnp.einsum(
        "prf,prd->pfd", hidden_act, full_cot, preferred_element_type=jnp.float32
    )
    grad_hidden = jnp.einsum(
        "prd,pfd->prf", full_cot, expert_down, preferred_element_type=jnp.float32
    )
    grad_pre_gate = (grad_hidden * pre_up * gate_sig * (1.0 + pre_gate * (1.0 - gate_sig))).astype(
        jnp.bfloat16
    )
    grad_pre_up = (grad_hidden * activated).astype(jnp.bfloat16)
    grad_expert_gate = jnp.einsum(
        "prd,prf->pdf", full_rows, grad_pre_gate, preferred_element_type=jnp.float32
    )
    grad_expert_up = jnp.einsum(
        "prd,prf->pdf", full_rows, grad_pre_up, preferred_element_type=jnp.float32
    )
    partial_grad = jnp.einsum(
        "prf,pdf->prd", grad_pre_gate, expert_gate, preferred_element_type=jnp.float32
    ) + jnp.einsum("prf,pdf->prd", grad_pre_up, expert_up, preferred_element_type=jnp.float32)
    me = lax.axis_index("sp")
    partial_rows = partial_grad.astype(jnp.bfloat16).reshape(local_count * group_count * capacity, -1)
    (other_core,) = exchange(1, ("cores", "core", partial_rows, part_width))
    chip_rows = (
        halves(partial_rows, part_width).astype(jnp.float32) + other_core.astype(jnp.float32)
    ).astype(jnp.bfloat16)
    chip_rows = jnp.swapaxes(
        chip_rows.reshape(local_count, group_count, capacity, half), 0, 1
    ).reshape(group_count, block_rows, half)
    (returned,) = exchange(2, ("rows", "sp", chip_rows))
    back = lax.rem(me - jnp.arange(group_count) + group_count, group_count)
    local_slots = jnp.arange(block_rows, dtype=jnp.int32)
    picks = jnp.sum(
        (slot_index.reshape(token_count, pick_count)[None, :, :, None])
        == (back[:, None] * block_rows + local_slots)[:, None, None, :],
        axis=2,
    ).astype(jnp.bfloat16)
    token_part = jnp.dot(
        picks[0],
        lax.dynamic_index_in_dim(chip_rows, me, 0, keepdims=False),
        preferred_element_type=jnp.float32,
    ) + jnp.einsum("kts,ksd->td", picks[1:], returned, preferred_element_type=jnp.float32)
    token_part = token_part.astype(jnp.bfloat16)
    (parts,) = exchange(3, ("columns", "z", token_part))
    own_part = lax.dynamic_slice_in_dim(
        token_part, lax.div(lax.axis_index("tp"), 2) * part_width, part_width, axis=1
    )
    moe_grad = own_part.astype(jnp.float32) + jnp.sum(parts.astype(jnp.float32), axis=0)
    mixer_cot = (cotangent.astype(jnp.float32) + moe_grad).astype(jnp.bfloat16)
    (mixer_z,) = exchange(8, ("gather", "z", mixer_cot))
    (mixer_other,) = exchange(9, ("swap", "core", mixer_z))
    full_mixer_cot = interleave(mixer_z, mixer_other, part_width)
    grad_mixed = jnp.dot(full_mixer_cot, out_proj, preferred_element_type=jnp.float32)
    grad_out_gate = (grad_mixed * conv_out).astype(jnp.bfloat16)
    grad_conv_out = grad_mixed * out_gate.astype(jnp.float32)
    rim_grad = padded(grad_conv_out, (("sp", 0),), 1)
    grad_conv_in = (
        rim_grad[2:] * conv_taps[0] + rim_grad[1:-1] * conv_taps[1] + rim_grad[:-2] * conv_taps[2]
    )
    grad_in_gate = (grad_conv_in * values.astype(jnp.float32)).astype(jnp.bfloat16)
    grad_values = (grad_conv_in * in_gate.astype(jnp.float32)).astype(jnp.bfloat16)
    columns = lax.all_to_all(full_mixer_cot, "sp", split_axis=1, concat_axis=0, tiled=True)
    grad_out_proj = lax.dot_general(
        columns,
        mixed_all.reshape(group_count * token_count, part_width),
        contract_rows,
        preferred_element_type=jnp.float32,
    )
    return (
        grad_out_gate,
        grad_in_gate,
        grad_values,
        grad_out_proj,
        grad_expert_gate,
        grad_expert_up,
        grad_expert_down,
    )


def solution(mesh):
    return jax.shard_map(
        body,
        mesh=mesh,
        in_specs=(
            P("sp", "tp"),
            P("sp", "tp"),
            P("sp", "tp"),
            P("sp", "tp"),
            P(None, "tp"),
            P(None, "tp"),
            P("sp", None),
            P("sp", None),
            P("sp", None, "tp"),
            P("sp", None, "tp"),
            P("sp", "tp", None),
            P("sp", "tp"),
        ),
        out_specs=(
            P("sp", "tp"),
            P("sp", "tp"),
            P("sp", "tp"),
            P("sp", "tp"),
            P("sp", None, "tp"),
            P("sp", None, "tp"),
            P("sp", "tp", None),
        ),
        check_vma=False,
    )
```

profile of v0, /device:TPU:0, one launch (start us, length us, event | category | flops | bytes accessed | tf_op | source)
XLA Modules:
  0.0 313.7 jit_solution(820335065723985253)
XLA Ops:
  0.6 1.2 convert_multiply_fusion.1
  1.9 4.9 %collective-permute-start = (f32[1,512]{1,0:T(1,128)S(1)}, f32[1,512]{1,0:T(1,128)S(1)}, u32[]{:S(2)}, u32[]{:S(2)}) collective-permute-start(f32[1,512]{1,0:T(1,128)S(1)} %get-tuple-element.37), channel_id=1, source_target_pairs={{0,8},{8,16},{16,24},{1,9},{9,17},{17,25},{2,10},{10,18},{18,26},{... | collective-permute-start | bytes 6152 | tf_op jit(solution)/shard_map/ppermute | solution.py:171
  6.8 1.3 collective-permute-start.1
  8.1 0.8 copy.36
  9.2 0.8 fusion.41
  10.0 1.2 reduce-window.6
  12.7 1.0 fusion.15
  13.7 0.9 select_reduce_fusion
  14.9 0.8 convert_element_type.88
  15.7 1.9 fusion.19.refs_1_
  17.6 24.5 %shard_map.171 = (bf16[256,2048]{1,0:T(8,128)(2,1)}, bf16[4,256,512]{2,1,0:T(8,128)(2,1)}) custom-call(bf16[256,512]{1,0:T(8,128)(2,1)} %refs_0_.2, bf16[256,512]{1,0:T(8,128)(2,1)} %fusion.19.refs_1_), custom_call_target="tpu_custom_call" | custom-call | tf_op jit(solution)/shard_map/pallas_call | solution.py:131
  42.1 4.0 %convolution_convert_fusion = bf16[768,2048]{1,0:T(8,128)(2,1)} fusion(pred[768,256]{1,0:T(8,128)(4,1)} %fusion.15, bf16[256,2048]{1,0:T(8,128)(2,1)} %get-tuple-element.13), kind=kOutput, calls=%fused_computation.6 | convolution fusion | flops 806879232 | bytes 4390912 | tf_op jit(solution)/shard_map/dot_general | solution.py:217
  46.1 41.5 %shard_map.172 = (bf16[256,2048]{1,0:T(8,128)(2,1)}, bf16[4,192,2048]{2,1,0:T(8,128)(2,1)}) custom-call(bf16[256,512]{1,0:T(8,128)(2,1)} %refs_0_.3, bf16[4,192,2048]{2,1,0:T(8,128)(2,1)} %bitcast.87), custom_call_target="tpu_custom_call" | custom-call | tf_op jit(solution)/shard_map/pallas_call | solution.py:131
  87.6 3.9 %multiply_convert_fusion = bf16[768,2048]{1,0:T(8,128)(2,1)} fusion(pred[768,256]{1,0:T(8,128)(4,1)S(1)} %copy-done.10, bf16[256,2048]{1,0:T(8,128)(2,1)} %get-tuple-element.14, f32[768]{0:T(1024)S(1)} %select_reduce_fusion), kind=kOutput, calls=%fused_computation.2 | convolution fusion | flops 808452096 | bytes 4393984 | tf_op jit(solution)/shard_map/dot_general | solution.py:224
  91.5 37.0 %shard_map.173 = (bf16[4,192,2048]{2,1,0:T(8,128)(2,1)}, bf16[768,2048]{1,0:T(8,128)(2,1)}) custom-call(bf16[4,192,2048]{2,1,0:T(8,128)(2,1)} %bitcast.92, bf16[768,2048]{1,0:T(8,128)(2,1)} %bitcast.90), custom_call_target="tpu_custom_call" | custom-call | tf_op jit(solution)/shard_map/pallas_call | solution.py:131
  128.5 6.1 %shard_map.174 = bf16[768,2048]{1,0:T(8,128)(2,1)} custom-call(bf16[768,2048]{1,0:T(8,128)(2,1)} %bitcast.91), custom_call_target="tpu_custom_call" | custom-call | tf_op jit(solution)/shard_map/pallas_call | solution.py:131
  134.5 5.3 %broadcast_select_fusion = (bf16[768,2048]{1,0:T(8,128)(2,1)S(1)}, bf16[768,2048]{1,0:T(8,128)(2,1)S(1)}, bf16[768,2048]{1,0:T(8,128)(2,1)S(1)}, bf16[768,2048]{1,0:T(8,128)(2,1)S(1)}) fusion(bf16[768,2048]{1,0:T(8,128)(2,1)} %get-tuple-element.17, pred[]{:T(512)S(6)} %eq.59, bf16[4,192,2048]{2,1,0:T(8,128)(2,1)} %get-tuple-element.15, ...), kind=kLoop, calls=%fused_computation.7 | loop fusion | flops 6291456 | bytes 25165824 | tf_op jit(solution)/shard_map/jit(_where)/select_n | solution.py:156
  141.3 1.8 fusion.5
  143.1 1.3 copy-done.4
  144.4 1.8 fusion.8
  146.3 1.0 copy-done.19
  147.2 2.0 multiply_convert_fusion.2
  149.3 3.9 %convolution_bitcast_fusion.1 = f32[1,4096,256]{2,1,0:T(8,128)} fusion(bf16[768,4096]{1,0:T(8,128)(2,1)S(1)} %slice_dynamic-update-slice_fusion, bf16[768,256]{1,0:T(8,128)(2,1)S(1)} %get-tuple-element.29), kind=kOutput, calls=%fused_computation.4 | convolution fusion | flops 1610612736 | bytes 10878976 | tf_op jit(solution)/shard_map/prd,prf->pdf/dot_general | solution.py:262
  153.2 1.8 fusion.3
  155.0 5.5 %add_convert_fusion.refs_0_ = bf16[768,4096]{1,0:T(8,128)(2,1)} fusion(f32[768,4096]{1,0:T(8,128)S(1)} %fusion.3, bf16[768,256]{1,0:T(8,128)(2,1)} %copy-done.16, bf16[1,4096,256]{2,1,0:T(8,128)(2,1)S(1)} %copy-done.4), kind=kOutput, calls=%fused_computation | convolution fusion | flops 1616904192 | bytes 21364736 | tf_op jit(solution)/shard_map/prf,pdf->prd/dot_general | solution.py:267
  160.5 6.1 %shard_map.175 = bf16[768,2048]{1,0:T(8,128)(2,1)} custom-call(bf16[768,4096]{1,0:T(8,128)(2,1)} %add_convert_fusion.refs_0_), custom_call_target="tpu_custom_call" | custom-call | tf_op jit(solution)/shard_map/pallas_call | solution.py:131
  166.6 2.3 constant_dynamic-slice_fusion.3
  169.5 2.2 add_convert_fusion.1
  171.6 37.5 %shard_map.176 = bf16[3,192,2048]{2,1,0:T(8,128)(2,1)} custom-call(bf16[4,192,2048]{2,1,0:T(8,128)(2,1)} %bitcast.88), custom_call_target="tpu_custom_call" | custom-call | tf_op jit(solution)/shard_map/pallas_call | solution.py:131
  209.2 2.7 convolution_bitcast_fusion.3
  211.8 2.6 fusion.refs_0_
  214.4 21.4 %shard_map.177 = bf16[3,256,512]{2,1,0:T(8,128)(2,1)} custom-call(bf16[256,2048]{1,0:T(8,128)(2,1)} %fusion.refs_0_), custom_call_target="tpu_custom_call" | custom-call | tf_op jit(solution)/shard_map/pallas_call | solution.py:131
  235.9 1.3 convert_reduce_fusion
  237.2 1.8 add_convert_fusion.2.refs_0_
  238.9 24.6 %shard_map.178.refs_0_ = bf16[256,2048]{1,0:T(8,128)(2,1)} custom-call(bf16[256,512]{1,0:T(8,128)(2,1)} %add_convert_fusion.2.refs_0_), custom_call_target="tpu_custom_call" | custom-call | tf_op jit(solution)/shard_map/pallas_call | solution.py:131
  263.6 3.1 shard_map.179
  266.6 1.7 broadcast_select_fusion.4
  268.3 0.7 slice_dynamic-update-slice_fusion.23
  274.1 4.1 %copy.40 = bf16[256,4096]{0,1:T(8,128)(2,1)} copy(bf16[256,4096]{1,0:T(8,128)(2,1)} %slice_dynamic-update-slice_fusion.16) | data formatting | bytes 4194304 | tf_op jit(solution)/shard_map/all_to_all | solution.py:309
  278.2 4.6 %all-to-all-start = ((bf16[256,4,1024]{0,2,1:T(8,128)(2,1)}), bf16[256,4,1024]{0,2,1:T(8,128)(2,1)}, u32[]{:S(2)}, u32[]{:S(2)}) async-start(bf16[256,4,1024]{0,2,1:T(8,128)(2,1)} %bitcast.15), calls=%async_computation | async-start | bytes 4194304 | tf_op jit(solution)/shard_map/all_to_all | solution.py:309
  282.8 5.0 %convert_multiply_fusion.3 = (f32[256,512]{1,0:T(8,128)S(1)}, bf16[256,512]{1,0:T(8,128)(2,1)}) fusion(bf16[256,512]{1,0:T(8,128)(2,1)S(1)} %copy-done.17, f32[512]{0:T(512)S(1)} %bitcast.99, f32[1,512]{1,0:T(1,128)S(1)} %collective-permute-done.1, f32[256,512]{1,0:T(8,128)S(1)} %convert_multiply_fusion.1, f32[512]{0:T(512)S(1)} %bitcast.102, ...), kind=kOutput, calls=%fused_computation.59 | convolution fusion | flops 1075183616 | bytes 7874560 | tf_op jit(solution)/shard_map/dot_general | solution.py:300
  287.8 1.3 collective-permute-start.2
  289.1 4.8 %collective-permute-start.3 = (f32[1,512]{1,0:T(1,128)S(1)}, f32[1,512]{1,0:T(1,128)S(1)}, u32[]{:S(2)}, u32[]{:S(2)}) collective-permute-start(f32[1,512]{1,0:T(1,128)S(1)} %get-tuple-element.34), channel_id=1, source_target_pairs={{0,8},{8,16},{16,24},{1,9},{9,17},{17,25},{2,10},{10,18},{18,26},{... | collective-permute-start | bytes 6152 | tf_op jit(solution)/shard_map/ppermute | solution.py:171
  294.0 6.7 %convolution_bitcast_fusion = f32[1,256,4096]{2,1,0:T(8,128)} fusion(bf16[768,4096]{1,0:T(8,128)(2,1)} %copy-done.2, f32[768,256]{1,0:T(8,128)S(1)} %copy-done.9, f32[768,256]{1,0:T(8,128)S(1)} %copy-done.7), kind=kOutput, calls=%fused_computation.3 | convolution fusion | flops 1611792384 | bytes 12058624 | tf_op jit(solution)/shard_map/prf,prd->pfd/dot_general | solution.py:249
  300.7 3.9 %convolution_bitcast_fusion.2 = f32[1,4096,256]{2,1,0:T(8,128)} fusion(bf16[768,4096]{1,0:T(8,128)(2,1)S(1)} %bitcast.94, bf16[768,256]{1,0:T(8,128)(2,1)S(1)} %copy-done.15), kind=kOutput, calls=%fused_computation.5 | convolution fusion | flops 1610612736 | bytes 10878976 | tf_op jit(solution)/shard_map/prd,prf->pdf/dot_general | solution.py:259
  304.7 3.7 %collective-permute-done.2 = f32[1,512]{1,0:T(1,128)S(1)} collective-permute-done((f32[1,512]{1,0:T(1,128)S(1)}, f32[1,512]{1,0:T(1,128)S(1)}, u32[]{:S(2)}, u32[]{:S(2)}) %collective-permute-start.2) | collective-permute-done | bytes 2080 | tf_op jit(solution)/shard_map/ppermute | solution.py:172
  308.4 1.0 fusion.20
  309.4 4.3 %fusion.12 = f32[1024,512]{1,0:T(8,128)} fusion(bf16[4,256,512]{2,1,0:T(8,128)(2,1)S(1)} %copy-done.20, bf16[256,4,1024]{0,2,1:T(8,128)(2,1)} %all-to-all-done), kind=kOutput, calls=%fused_computation.25 | convolution fusion | flops 1073741824 | bytes 5242880 | tf_op jit(solution)/shard_map/dot_general | solution.py:310
  (87 shorter events, 9.0 us)
Async XLA Ops:
  0.6 140.6 %copy-start = (bf16[1,4096,256]{2,1,0:T(8,128)(2,1)S(1)}, bf16[1,4096,256]{2,1,0:T(8,128)(2,1)}, u32[]{:S(2)}) copy-start(bf16[1,4096,256]{2,1,0:T(8,128)(2,1)} %param.20) | copy-start | bytes 6291460
  1.9 13.8 %collective-permute-start = (f32[1,512]{1,0:T(1,128)S(1)}, f32[1,512]{1,0:T(1,128)S(1)}, u32[]{:S(2)}, u32[]{:S(2)}) collective-permute-start(f32[1,512]{1,0:T(1,128)S(1)} %get-tuple-element.37), channel_id=1, source_target_pairs={{0,8},{8,16},{16,24},{1,9},{9,17},{17,25},{2,10},{10,18},{18,26},{... | collective-permute-start | bytes 6152 | tf_op jit(solution)/shard_map/ppermute | solution.py:171
  6.8 8.9 %collective-permute-start.1 = (f32[1,512]{1,0:T(1,128)S(1)}, f32[1,512]{1,0:T(1,128)S(1)}, u32[]{:S(2)}, u32[]{:S(2)}) collective-permute-start(f32[1,512]{1,0:T(1,128)S(1)} %get-tuple-element.38), channel_id=1, source_target_pairs={{8,0},{16,8},{24,16},{9,1},{17,9},{25,17},{10,2},{18,10},{26,18},{... | collective-permute-start | bytes 6152 | tf_op jit(solution)/shard_map/ppermute | solution.py:172
  46.0 41.5 %copy-start.10 = (pred[768,256]{1,0:T(8,128)(4,1)S(1)}, pred[768,256]{1,0:T(8,128)(4,1)}, u32[]{:S(2)}) copy-start(pred[768,256]{1,0:T(8,128)(4,1)} %fusion.15) | copy-start | bytes 589828
  140.5 5.7 %copy-start.2 = (bf16[768,4096]{1,0:T(8,128)(2,1)}, bf16[768,4096]{1,0:T(8,128)(2,1)S(1)}, u32[]{:S(2)}) copy-start(bf16[768,4096]{1,0:T(8,128)(2,1)S(1)} %slice_dynamic-update-slice_fusion.8) | copy-start | bytes 18874372
  141.3 8.0 %copy-start.18 = (bf16[768,4096]{1,0:T(8,128)(2,1)}, bf16[768,4096]{1,0:T(8,128)(2,1)S(1)}, u32[]{:S(2)}) copy-start(bf16[768,4096]{1,0:T(8,128)(2,1)S(1)} %slice_dynamic-update-slice_fusion) | copy-start | bytes 18874372
  141.3 3.2 %copy-start.4 = (bf16[1,4096,256]{2,1,0:T(8,128)(2,1)S(1)}, bf16[1,4096,256]{2,1,0:T(8,128)(2,1)}, u32[]{:S(2)}) copy-start(bf16[1,4096,256]{2,1,0:T(8,128)(2,1)} %param.21) | copy-start | bytes 6291460
  144.4 1.8 copy-start.6
  144.4 2.8 copy-start.19
  147.2 2.0 copy-start.8
  149.2 4.0 %copy-start.16 = (bf16[768,256]{1,0:T(8,128)(2,1)}, bf16[768,256]{1,0:T(8,128)(2,1)S(1)}, u32[]{:S(2)}) copy-start(bf16[768,256]{1,0:T(8,128)(2,1)S(1)} %get-tuple-element.29) | copy-start | bytes 1179652
  149.2 4.0 %copy-start.14 = (bf16[768,256]{1,0:T(8,128)(2,1)}, bf16[768,256]{1,0:T(8,128)(2,1)S(1)}, u32[]{:S(2)}) copy-start(bf16[768,256]{1,0:T(8,128)(2,1)S(1)} %get-tuple-element.30) | copy-start | bytes 1179652
  166.6 2.9 copy-start.3
  171.6 37.5 %copy-start.5 = (bf16[4,256,192]{1,2,0:T(8,128)(2,1)S(1)}, bf16[4,256,192]{1,2,0:T(8,128)(2,1)}, u32[]{:S(2)}) copy-start(bf16[4,256,192]{1,2,0:T(8,128)(2,1)} %convert_element_type.88) | copy-start | bytes 1179652
  211.8 25.3 %copy-start.11 = (bf16[256,512]{1,0:T(8,128)(2,1)S(1)}, bf16[256,512]{1,0:T(8,128)(2,1)}, u32[]{:S(2)}) copy-start(bf16[256,512]{1,0:T(8,128)(2,1)} %refs_0_.3) | copy-start | bytes 786436
  278.2 4.6 %copy-start.17 = (bf16[256,512]{1,0:T(8,128)(2,1)S(1)}, bf16[256,512]{1,0:T(8,128)(2,1)}, u32[]{:S(2)}) copy-start(bf16[256,512]{1,0:T(8,128)(2,1)} %param.13) | copy-start | bytes 786436
  278.2 31.2 %all-to-all-start = ((bf16[256,4,1024]{0,2,1:T(8,128)(2,1)}), bf16[256,4,1024]{0,2,1:T(8,128)(2,1)}, u32[]{:S(2)}, u32[]{:S(2)}) async-start(bf16[256,4,1024]{0,2,1:T(8,128)(2,1)} %bitcast.15), calls=%async_computation | async-start | bytes 4194304 | tf_op jit(solution)/shard_map/all_to_all | solution.py:309
  282.8 11.1 %copy-start.7 = (f32[768,256]{1,0:T(8,128)S(1)}, f32[768,256]{1,0:T(8,128)}, u32[]{:S(2)}) copy-start(f32[768,256]{1,0:T(8,128)} %copy-done.6) | copy-start | bytes 2359300
  282.8 11.1 %copy-start.9 = (f32[768,256]{1,0:T(8,128)S(1)}, f32[768,256]{1,0:T(8,128)}, u32[]{:S(2)}) copy-start(f32[768,256]{1,0:T(8,128)} %copy-done.8) | copy-start | bytes 2359300
  287.8 20.5 %collective-permute-start.2 = (f32[1,512]{1,0:T(1,128)S(1)}, f32[1,512]{1,0:T(1,128)S(1)}, u32[]{:S(2)}, u32[]{:S(2)}) collective-permute-start(f32[1,512]{1,0:T(1,128)S(1)} %get-tuple-element.33), channel_id=1, source_target_pairs={{8,0},{16,8},{24,16},{9,1},{17,9},{25,17},{10,2},{18,10},{26,18},{... | collective-permute-start | bytes 6152 | tf_op jit(solution)/shard_map/ppermute | solution.py:172
  289.1 11.6 %slice-start = ((s8[6291456]{0:T(1024)(128)(4,1)}), s8[4194304]{0:T(1024)(128)(4,1)S(1)}, s32[]{:S(2)}) async-start(s8[6291456]{0:T(1024)(128)(4,1)} %bitcast.93), calls=%async_computation.1 | async-start | bytes 8388608
  289.1 11.5 %copy-start.15 = (bf16[768,256]{1,0:T(8,128)(2,1)S(1)}, bf16[768,256]{1,0:T(8,128)(2,1)}, u32[]{:S(2)}) copy-start(bf16[768,256]{1,0:T(8,128)(2,1)} %copy-done.14) | copy-start | bytes 1179652
  289.1 11.5 %slice-start.1 = ((s8[6291456]{0:T(1024)(128)(4,1)}), s8[2097152]{0:T(1024)(128)(4,1)S(1)}, s32[]{:S(2)}) async-start(s8[6291456]{0:T(1024)(128)(4,1)} %bitcast.93), calls=%async_computation.2 | async-start | bytes 4194304
  289.1 19.2 %collective-permute-start.3 = (f32[1,512]{1,0:T(1,128)S(1)}, f32[1,512]{1,0:T(1,128)S(1)}, u32[]{:S(2)}, u32[]{:S(2)}) collective-permute-start(f32[1,512]{1,0:T(1,128)S(1)} %get-tuple-element.34), channel_id=1, source_target_pairs={{0,8},{8,16},{16,24},{1,9},{9,17},{17,25},{2,10},{10,18},{18,26},{... | collective-permute-start | bytes 6152 | tf_op jit(solution)/shard_map/ppermute | solution.py:171
  300.7 7.7 %copy-start.12 = (bf16[256,512]{1,0:T(8,128)(2,1)S(1)}, bf16[256,512]{1,0:T(8,128)(2,1)}, u32[]{:S(2)}) copy-start(bf16[256,512]{1,0:T(8,128)(2,1)} %param.15) | copy-start | bytes 786436
  300.7 7.7 %copy-start.13 = (bf16[256,512]{1,0:T(8,128)(2,1)S(1)}, bf16[256,512]{1,0:T(8,128)(2,1)}, u32[]{:S(2)}) copy-start(bf16[256,512]{1,0:T(8,128)(2,1)} %param.14) | copy-start | bytes 786436
  300.7 8.7 %copy-start.20 = (bf16[4,256,512]{2,1,0:T(8,128)(2,1)S(1)}, bf16[4,256,512]{2,1,0:T(8,128)(2,1)}, u32[]{:S(2)}) copy-start(bf16[4,256,512]{2,1,0:T(8,128)(2,1)} %get-tuple-element.18) | copy-start | bytes 3145732
  309.4 4.3 %copy-start.1 = (bf16[1,4096,256]{2,1,0:T(8,128)(2,1)S(1)}, bf16[1,4096,256]{2,1,0:T(8,128)(2,1)}, u32[]{:S(2)}) copy-start(bf16[1,4096,256]{2,1,0:T(8,128)(2,1)} %param.20) | copy-start | bytes 6291460
where the time goes:
time: 317 us; the launch traced here: 314 us
  Pallas kernels  202 us (64%)
  matrix products  49.9 us (16%)
  other arithmetic  21.5 us (7%)
  local copies, waits for them, and re-layouts  18.8 us (6%)
  starting transfers between devices  16.9 us (5%)
  waiting for transfers between devices  3.72 us (1%)
    pallas_call x9, Pallas kernels, exchange(): pl.pallas_call(kernel, out_shape=shapes, in_specs=[pl.BlockSpec(memory_sp...  202 us
    unnamed x68, local copies, waits for them, and re-layouts  9.91 us
    ppermute x2, starting transfers between devices, padded(): before = lax.ppermute(last, axis, up)  9.68 us
    select_n x2, other arithmetic, interleave(): jnp.where(core == 0, other, own)  6.93 us
    dot_general x1, matrix products, body(): jnp.einsum('prf,prd->pfd', hidden_act, full_cot, preferred_element_type=j...  6.68 us
  transfers between devices with their start and end apart: 5, of which 1 were waited for; matrix products, arithmetic and copies ran while one was open for 8% of the time, Pallas kernels for 0%

commit v1 on v0

--- a/solution.py
+++ b/solution.py
@@ -324,9 +324,481 @@
     )
 
 
+def flip(index, bits):
+    high, low = (lax.div(index, 2), lax.rem(index, 2))
+    bit_high, bit_low = (lax.div(bits, 2), lax.rem(bits, 2)) if not isinstance(bits, int) else (bits // 2, bits % 2)
+    high = high + bit_high - 2 * high * bit_high
+    low = low + bit_low - 2 * low * bit_low
+    return 2 * high + low
+
+
+def place():
+    sp, tp = (lax.axis_index("sp"), lax.axis_index("tp"))
+    return sp, lax.div(tp, 2), lax.rem(tp, 2)
+
+
+def greet(devices):
+    barrier = pltpu.get_barrier_semaphore()
+    for device in devices:
+        pl.semaphore_signal(barrier, inc=1, device_id=device, device_id_type=MESH)
+    pl.semaphore_wait(barrier, len(devices))
+
+
+def remote(source, target, send_sem, recv_sem, device):
+    return pltpu.make_async_remote_copy(
+        src_ref=source,
+        dst_ref=target,
+        send_sem=send_sem,
+        recv_sem=recv_sem,
+        device_id=device,
+        device_id_type=MESH,
+    )
+
+
+def dot_nt(a, b):
+    return lax.dot_general(a, b, (((1,), (1,)), ((), ())), preferred_element_type=jnp.float32)
+
+
+def dot_nn(a, b):
+    return jnp.dot(a, b, preferred_element_type=jnp.float32)
+
+
+def experts_kernel(tokens, width, hidden):
+    groups, layers = (4, 4)
+    parts = 2 * layers
+    rows_all = groups * tokens
+
+    def kernel(
+        x_hbm, c_hbm, route, wg_hbm, wu_hbm, wd_hbm,
+        xf, cf, g_out, u_out, h_out, mixer_out,
+        xc, w, wd, wp, acc, a, hb, wrow, own_sum, result,
+        sd, sx, sy, sz, rd, rx, ry, rz,
+        load, xc_send, xc_recv, wr_send, wr_recv, wp_send, wp_recv, a_send, a_recv,
+        rs_send, rs_recv, out_sem, col_sem,
+    ):
+        sp, z, c = place()
+        tp = 2 * z + c
+        xn, yn, dn = (flip(sp, 1), flip(sp, 2), flip(sp, 3))
+        near = 1 - c
+        partner = (sp, 2 * z + near)
+        x_dev, y_dev, d_dev = ((xn, tp), (yn, tp), (dn, tp))
+
+        def z_dev(k):
+            return (sp, 2 * flip(z, k) + c)
+
+        def rows(s):
+            return pl.ds(pl.multiple_of(s * tokens, tokens), tokens)
+
+        def blk(t, s, part):
+            return xc.at[t, part, rows(s)]
+
+        loads = [
+            pltpu.make_async_copy(x_hbm, blk(0, sp, tp), load.at[0]),
+            pltpu.make_async_copy(c_hbm, blk(1, sp, tp), load.at[1]),
+            pltpu.make_async_copy(wg_hbm, w.at[0], load.at[2]),
+            pltpu.make_async_copy(wu_hbm, w.at[1], load.at[3]),
+            pltpu.make_async_copy(route.at[sp], wrow.at[sp], load.at[4]),
+        ]
+        for part in range(parts):
+            loads.append(
+                pltpu.make_async_copy(
+                    wd_hbm.at[:, pl.ds(part * width, width)], wd.at[part], load.at[5 + part]
+                )
+            )
+        for copy in loads:
+            copy.start()
+        greet([partner, z_dev(1), z_dev(2), z_dev(3), x_dev, y_dev, d_dev])
+        loads[0].wait()
+        loads[1].wait()
+
+        def pass_on(t, s, part, slot, device):
+            return remote(
+                blk(t, s, part), blk(t, s, part), xc_send.at[t, slot], xc_recv.at[t, s, part], device
+            )
+
+        def arrive(t, s, part):
+            pass_on(t, s, part, 0, partner).wait_recv()
+
+        for k in (1, 2, 3):
+            for t in (0, 1):
+                pass_on(t, sp, tp, 11 + k, z_dev(k)).start()
+            if k == 1:
+                for t in (0, 1):
+                    pass_on(t, sp, tp, 4, x_dev).start()
+                    pass_on(t, sp, tp, 8, y_dev).start()
+                    pass_on(t, sp, tp, 0, partner).start()
+        route_copies = []
+        for i, (s, device) in enumerate(((xn, x_dev), (yn, y_dev), (dn, d_dev))):
+            copy = remote(route.at[s], wrow.at[sp], wr_send.at[i], wr_recv.at[i], device)
+            copy.start()
+            route_copies.append(copy)
+        for copy in loads[2:]:
+            copy.wait()
+        weight_copies = []
+        for j in (0, 1):
+            for part in range(layers):
+                copy = remote(
+                    w.at[j, 2 * part + near], wp.at[j, part], wp_send.at[j, part], wp_recv.at[j, part], partner
+                )
+                copy.start()
+                weight_copies.append(copy)
+        acc[...] = jnp.zeros_like(acc)
+
+        def column_copy(t, part):
+            cols = pl.ds(pl.multiple_of(part * width, width), width)
+            target = (xf, cf)[t]
+            return pltpu.make_async_copy(xc.at[t, part], target.at[:, cols], col_sem.at[t, part])
+
+        def multiply(t, part):
+            @pl.when(t == 0)
+            def _():
+                column_copy(0, part).start()
+
+                @pl.loop(0, groups)
+                def _(s):
+                    tile = xc[0, part, rows(s), :]
+                    acc[0, rows(s), :] += dot_nn(tile, w[0, part])
+                    acc[1, rows(s), :] += dot_nn(tile, w[1, part])
+
+            @pl.when(t == 1)
+            def _():
+                column_copy(1, part).start()
+
+                @pl.loop(0, groups)
+                def _(s):
+                    acc[2, rows(s), :] += dot_nt(xc[1, part, rows(s), :], wd[part])
+
+        def step(i, carry):
+            r, t = (lax.div(i, 2), lax.rem(i, 2))
+
+            @pl.when(i < 6)
+            def _():
+                part = 2 * flip(z, r + 1) + c
+                arrive(t, sp, part)
+                pass_on(t, sp, part, 5 + r, x_dev).start()
+                pass_on(t, sp, part, 9 + r, y_dev).start()
+                pass_on(t, sp, part, 1 + r, partner).start()
+
+            @pl.when(i < 8)
+            def _():
+                part = 2 * flip(z, r) + c
+                even = lax.rem(r, 2) == 0
+                arrive(t, xn, part)
+
+                @pl.when(even)
+                def _():
+                    pass_on(t, xn, part, 27 + r, y_dev).start()
+
+                pass_on(t, xn, part, 15 + r, partner).start()
+                arrive(t, yn, part)
+
+                @pl.when(lax.rem(r, 2) == 1)
+                def _():
+                    pass_on(t, yn, part, 27 + r, x_dev).start()
+
+                pass_on(t, yn, part, 19 + r, partner).start()
+
+            @pl.when((i >= 2) & (i < 10))
+            def _():
+                part = 2 * flip(z, r - 1) + c
+                arrive(t, dn, part)
+                pass_on(t, dn, part, 22 + r, partner).start()
+
+            @pl.when(i >= 3)
+            def _():
+                j = i - 3
+                kj, tj = (lax.div(j, 2), lax.rem(j, 2))
+                layer = flip(z, kj)
+                multiply(tj, 2 * layer + c)
+                for s in range(groups):
+                    arrive(tj, s, 2 * layer + near)
+                multiply(tj, 2 * layer + near)
+
+            return carry
+
+        lax.fori_loop(0, 11, step, 0)
+
+        for copy in route_copies:
+            copy.wait()
+        for copy in weight_copies:
+            copy.wait()
+        half = 128
+        eye = lax.broadcasted_iota(jnp.int32, (half, half), 0) == lax.broadcasted_iota(
+            jnp.int32, (half, half), 1
+        )
+        a_copies = []
+        for i, s in enumerate((dn, xn, yn, sp)):
+            columns = []
+            for h in range(tokens // half):
+                line = jnp.broadcast_to(wrow[s, 0:1, h * half : (h + 1) * half], (half, half))
+                columns.append(jnp.sum(jnp.where(eye, line, 0.0), axis=1, keepdims=True))
+
+            for h in range(tokens // half):
+                here = pl.ds(pl.multiple_of(s * tokens + h * half, half), half)
+                gate, up = (acc[0, here, :], acc[1, here, :])
+                back = acc[2, here, :] * columns[h]
+                sig = jax.nn.sigmoid(gate)
+                act = gate * sig
+                hb[here, :] = (act * up * columns[h]).astype(jnp.bfloat16)
+                a[0, here, :] = (back * up * sig * (1.0 + gate * (1.0 - sig))).astype(jnp.bfloat16)
+                a[1, here, :] = (back * act).astype(jnp.bfloat16)
+            for j in (0, 1):
+                copy = remote(
+                    a.at[j, rows(s)], a.at[2 + j, rows(s)], a_send.at[j, i], a_recv.at[j, i], partner
+                )
+                copy.start()
+                a_copies.append(copy)
+        outs = [
+            pltpu.make_async_copy(a.at[0], g_out, out_sem.at[0]),
+            pltpu.make_async_copy(a.at[1], u_out, out_sem.at[1]),
+            pltpu.make_async_copy(hb, h_out, out_sem.at[2]),
+        ]
+        for copy in outs:
+            copy.start()
+
+        def partial(s, k, finish):
+            layer = flip(z, k)
+            part = 2 * layer + c
+            tile = 256
+
+            @pl.loop(0, width // tile)
+            def _(n):
+                cols = pl.ds(pl.multiple_of(n * tile, tile), tile)
+                value = dot_nt(a[0, rows(s), :], w[0, part, cols, :])
+                value += dot_nt(a[1, rows(s), :], w[1, part, cols, :])
+                value += dot_nt(a[2, rows(s), :], wp[0, layer, cols, :])
+                value += dot_nt(a[3, rows(s), :], wp[1, layer, cols, :])
+                finish(cols, value)
+
+        rs_copies = []
+
+        def ship(kind, k, source, target, device):
+            copy = remote(source.at[k], target.at[k], rs_send.at[kind, k], rs_recv.at[kind, k], device)
+            copy.start()
+            rs_copies.append(copy)
+            return copy
+
+        def landed(kind, k, source, target):
+            remote(source.at[k], target.at[k], rs_send.at[kind, k], rs_recv.at[kind, k], partner).wait_recv()
+
+        def store_in(buffer, k):
+            def finish(cols, value):
+                buffer[k, :, cols] = value.astype(jnp.bfloat16)
+
+            return finish
+
+        def merge_in(buffer, other, k):
+            def finish(cols, value):
+                buffer[k, :, cols] = (value + other[k, :, cols].astype(jnp.float32)).astype(jnp.bfloat16)
+
+            return finish
+
+        def far(even, odd):
+            partial(dn, even, store_in(sd, even))
+            ship(0, even, sd, rd, x_dev)
+            partial(dn, odd, store_in(sd, odd))
+            ship(0, odd, sd, rd, y_dev)
+
+        def direct(even, odd):
+            partial(xn, even, store_in(sx, even))
+            ship(1, even, sx, rx, x_dev)
+            partial(yn, odd, store_in(sy, odd))
+            ship(2, odd, sy, ry, y_dev)
+
+        def merged(even, odd):
+            landed(0, even, sd, rd)
+            partial(yn, even, merge_in(sy, rd, even))
+            ship(2, even, sy, ry, y_dev)
+            landed(0, odd, sd, rd)
+            partial(xn, odd, merge_in(sx, rd, odd))
+            ship(1, odd, sx, rx, x_dev)
+
+        def collect(k):
+            landed(1, k, sx, rx)
+            landed(2, k, sy, ry)
+
+            def finish(cols, value):
+                total = value + rx[k, :, cols].astype(jnp.float32) + ry[k, :, cols].astype(jnp.float32)
+                if k:
+                    sz[k, :, cols] = total.astype(jnp.bfloat16)
+                else:
+                    own_sum[:, cols] = total
+
+            partial(sp, k, finish)
+            if k:
+                ship(3, k, sz, rz, z_dev(k))
+
+        for i in range(2):
+            for j in (0, 1):
+                a_copies[2 * i + j].wait_recv()
+            if i == 0:
+                far(2, 3)
+        for copy in a_copies[4:]:
+            copy.wait_recv()
+        direct(2, 3)
+        merged(2, 3)
+        far(0, 1)
+        direct(0, 1)
+        collect(3)
+        collect(2)
+        merged(0, 1)
+        collect(1)
+        collect(0)
+        for k in (3, 2, 1):
+            landed(3, k, sz, rz)
+
+        @pl.loop(0, width // 256)
+        def _(n):
+            cols = pl.ds(pl.multiple_of(n * 256, 256), 256)
+            total = own_sum[:, cols] + xc[1, tp, rows(sp), cols].astype(jnp.float32)
+            for k in (1, 2, 3):
+                total += rz[k, :, cols].astype(jnp.float32)
+            result[:, cols] = total.astype(jnp.bfloat16)
+
+        last = pltpu.make_async_copy(result, mixer_out, out_sem.at[3])
+        last.start()
+        for copy in rs_copies + a_copies:
+            copy.wait_send()
+        for t in (0, 1):
+
+            @pl.loop(0, 31)
+            def _(slot):
+                pass_on(t, sp, tp, slot, partner).wait_send()
+
+            @pl.loop(0, parts)
+            def _(part):
+                column_copy(t, part).wait()
+
+        for copy in outs:
+            copy.wait()
+        last.wait()
+
+    block_shape = (layers, tokens, width)
+    shapes = [
+        jax.ShapeDtypeStruct((rows_all, parts * width), jnp.bfloat16),
+        jax.ShapeDtypeStruct((rows_all, parts * width), jnp.bfloat16),
+        jax.ShapeDtypeStruct((rows_all, hidden), jnp.bfloat16),
+        jax.ShapeDtypeStruct((rows_all, hidden), jnp.bfloat16),
+        jax.ShapeDtypeStruct((rows_all, hidden), jnp.bfloat16),
+        jax.ShapeDtypeStruct((tokens, width), jnp.bfloat16),
+    ]
+    half = jnp.bfloat16
+    return pl.pallas_call(
+        kernel,
+        out_shape=shapes,
+        in_specs=[pl.BlockSpec(memory_space=pl.ANY)] * 6,
+        out_specs=[pl.BlockSpec(memory_space=pl.ANY)] * 6,
+        scratch_shapes=[
+            pltpu.VMEM((2, parts, rows_all, width), half),
+            pltpu.VMEM((2, parts, width, hidden), half),
+            pltpu.VMEM((parts, hidden, width), half),
+            pltpu.VMEM((2, layers, width, hidden), half),
+            pltpu.VMEM((3, rows_all, hidden), jnp.float32),
+            pltpu.VMEM((4, rows_all, hidden), half),
+            pltpu.VMEM((rows_all, hidden), half),
+            pltpu.VMEM((groups, 8, tokens), jnp.float32),
+            pltpu.VMEM((tokens, width), jnp.float32),
+            pltpu.VMEM((tokens, width), half),
+        ]
+        + [pltpu.VMEM(block_shape, half)] * 8
+        + [
+            pltpu.SemaphoreType.DMA((5 + parts,)),
+            pltpu.SemaphoreType.DMA((2, 31)),
+            pltpu.SemaphoreType.DMA((2, groups, parts)),
+            pltpu.SemaphoreType.DMA((3,)),
+            pltpu.SemaphoreType.DMA((3,)),
+            pltpu.SemaphoreType.DMA((2, layers)),
+            pltpu.SemaphoreType.DMA((2, layers)),
+            pltpu.SemaphoreType.DMA((2, groups)),
+            pltpu.SemaphoreType.DMA((2, groups)),
+            pltpu.SemaphoreType.DMA((4, layers)),
+            pltpu.SemaphoreType.DMA((4, layers)),
+            pltpu.SemaphoreType.DMA((4,)),
+            pltpu.SemaphoreType.DMA((2, parts)),
+        ],
+        compiler_params=pltpu.CompilerParams(
+            collective_id=10, has_side_effects=True, vmem_limit_bytes=60 * 1024 * 1024
+        ),
+    )
+
+
+def near_body(
+    moe_input,
+    out_gate,
+    in_gate,
+    values,
+    conv_taps,
+    out_proj,
+    route_ids,
+    route_gates,
+    expert_gate,
+    expert_up,
+    expert_down,
+    cotangent,
+):
+    token_count, part_width = moe_input.shape
+    group_count = lax.axis_size("sp")
+    hidden = expert_gate.shape[2]
+    part_count = lax.axis_size("tp")
+    contract_rows = (((0,), (0,)), ((), ()))
+    chosen = route_ids[None, :, :] == jnp.arange(group_count, dtype=jnp.int32)[:, None, None]
+    weights = jnp.sum(jnp.where(chosen, route_gates[None, :, :], 0.0), axis=2)
+    route = jnp.broadcast_to(weights[:, None, :], (group_count, 8, token_count))
+    x_all, cot_all, grad_pre_gate, grad_pre_up, hidden_act, mixer_cot = experts_kernel(
+        token_count, part_width, hidden
+    )(
+        moe_input,
+        cotangent,
+        route,
+        expert_gate.reshape(part_count, part_width, hidden),
+        expert_up.reshape(part_count, part_width, hidden),
+        expert_down[0],
+    )
+
+    def outer(a, b):
+        return lax.dot_general(a, b, contract_rows, preferred_element_type=jnp.float32)[None]
+
+    grad_expert_gate = outer(x_all, grad_pre_gate)
+    grad_expert_up = outer(x_all, grad_pre_up)
+    grad_expert_down = outer(hidden_act, cot_all)
+    conv_in = in_gate.astype(jnp.float32) * values.astype(jnp.float32)
+    rimmed = padded(conv_in, (("sp", 0),), 1)
+    conv_out = rimmed[:-2] * conv_taps[0] + rimmed[1:-1] * conv_taps[1] + rimmed[2:] * conv_taps[2]
+    mixed = (out_gate.astype(jnp.float32) * conv_out).astype(jnp.bfloat16)
+    mixer_z, mixed_all = exchange(8, ("gather", "z", mixer_cot), ("stack", "sp", mixed))
+    (mixer_other,) = exchange(9, ("swap", "core", mixer_z))
+    full_mixer_cot = interleave(mixer_z, mixer_other, part_width)
+    grad_mixed = jnp.dot(full_mixer_cot, out_proj, preferred_element_type=jnp.float32)
+    grad_out_gate = (grad_mixed * conv_out).astype(jnp.bfloat16)
+    grad_conv_out = grad_mixed * out_gate.astype(jnp.float32)
+    rim_grad = padded(grad_conv_out, (("sp", 0),), 1)
+    grad_conv_in = (
+        rim_grad[2:] * conv_taps[0] + rim_grad[1:-1] * conv_taps[1] + rim_grad[:-2] * conv_taps[2]
+    )
+    grad_in_gate = (grad_conv_in * values.astype(jnp.float32)).astype(jnp.bfloat16)
+    grad_values = (grad_conv_in * in_gate.astype(jnp.float32)).astype(jnp.bfloat16)
+    columns = lax.all_to_all(full_mixer_cot, "sp", split_axis=1, concat_axis=0, tiled=True)
+    grad_out_proj = lax.dot_general(
+        columns,
+        mixed_all.reshape(group_count * token_count, part_width),
+        contract_rows,
+        preferred_element_type=jnp.float32,
+    )
+    return (
+        grad_out_gate,
+        grad_in_gate,
+        grad_values,
+        grad_out_proj,
+        grad_expert_gate,
+        grad_expert_up,
+        grad_expert_down,
+    )
+
+
 def solution(mesh):
+    square = mesh.shape["sp"] == 4 and mesh.shape["tp"] == 8
     return jax.shard_map(
-        body,
+        near_body if square else body,
         mesh=mesh,
         in_specs=(
             P("sp", "tp"),

time: 317 us -> 228 us (0.72)
  Pallas kernels: 202 us -> 163 us
  matrix products: 49.9 us -> 29 us
  other arithmetic: 21.5 us -> 5.14 us
  local copies, waits for them, and re-layouts: 18.8 us -> 3.29 us
  waiting for transfers between devices: 3.72 us -> 7.43 us
    pallas_call x9 -> x2, Pallas kernels: 202 us -> 26 us  [exchange(): pl.pallas_call(kernel, out_shape=shapes, in_specs=[pl.BlockSpec(memory_sp...]
    pallas_call x0 -> x1, Pallas kernels: none -> 137 us  [near_body(): experts_kernel(token_count, part_width, hidden)]
    dot_general x14 -> x5, matrix products: 49.9 us -> 29 us  [the longest x3 20.5 us: outer(): lax.dot_general(a, b, contract_rows, preferred_element_type=jnp.float32)]
    unnamed x68 -> x25, local copies, waits for them, and re-layouts: 9.91 us -> 0.18 us
    convert_element_type x6 -> x2, other arithmetic: 7.63 us -> 1.96 us  [the longest x1 1.04 us: near_body(): (grad_conv_in * in_gate.astype(jnp.float32)).astype(jnp.bfloat16)]
    select_n x2 -> x1, other arithmetic: 6.93 us -> 1.37 us  [interleave(): jnp.where(core == 0, other, own)]
    ppermute x2, waiting for transfers between devices: 3.71 us -> 7.42 us  [padded(): after = lax.ppermute(initial, axis, down)]
  transfers between devices with their start and end apart: 5 -> 5, of which waited for: 1 -> 1; matrix products, arithmetic and copies ran while one was open for 8% -> 12% of each run, Pallas kernels for 0% -> 61%
where the time goes in v1:
time: 228 us; the launch traced here: 226 us
  Pallas kernels  163 us (71%)
  matrix products  29 us (13%)
  starting transfers between devices  16.7 us (7%)
  waiting for transfers between devices  7.43 us (3%)
  other arithmetic  5.14 us (2%)
  local copies, waits for them, and re-layouts  3.29 us (1%)
    pallas_call x1, Pallas kernels, near_body(): experts_kernel(token_count, part_width, hidden)  137 us
    pallas_call x2, Pallas kernels, exchange(): pl.pallas_call(kernel, out_shape=shapes, in_specs=[pl.BlockSpec(memory_sp...  26 us
    dot_general x3, matrix products, outer(): lax.dot_general(a, b, contract_rows, preferred_element_type=jnp.float32)  20.5 us
    ppermute x2, starting transfers between devices, padded(): before = lax.ppermute(last, axis, up)  9.42 us
    ppermute x2, waiting for transfers between devices, padded(): after = lax.ppermute(initial, axis, down)  7.42 us
    all_to_all x1, starting transfers between devices, near_body(): lax.all_to_all(full_mixer_cot, 'sp', split_axis=1, concat_axis=0, tiled=T...  4.69 us
  transfers between devices with their start and end apart: 5, of which 1 were waited for; matrix products, arithmetic and copies ran while one was open for 12% of the time, Pallas kernels for 61%

profile of v1, /device:TPU:0, one launch (start us, length us, event | category | flops | bytes accessed | tf_op | source)
XLA Modules:
  0.0 225.8 jit_solution(14094046079524529375)
XLA Ops:
  0.6 1.1 convert_multiply_fusion.1
  1.7 4.9 %collective-permute-start = (f32[1,512]{1,0:T(1,128)S(1)}, f32[1,512]{1,0:T(1,128)S(1)}, u32[]{:S(2)}, u32[]{:S(2)}) collective-permute-start(f32[1,512]{1,0:T(1,128)S(1)} %get-tuple-element.31), channel_id=1, source_target_pairs={{0,8},{8,16},{16,24},{1,9},{9,17},{17,25},{2,10},{10,18},{18,26},{... | collective-permute-start | bytes 6152 | tf_op jit(solution)/shard_map/ppermute | solution.py:171
  6.6 1.3 collective-permute-start.1
  7.9 0.7 select_reduce_fusion
  8.6 0.6 broadcast_in_dim.32.route
  9.3 137.4 %shard_map.171 = (bf16[1024,4096]{1,0:T(8,128)(2,1)}, bf16[1024,4096]{1,0:T(8,128)(2,1)}, bf16[1024,256]{1,0:T(8,128)(2,1)}, bf16[1024,256]{1,0:T(8,128)(2,1)}, ...) custom-call(bf16[256,512]{1,0:T(8,128)(2,1)} %x_hbm.1, bf16[256,512]{1,0:T(8,128)(2,1)} %c_hbm.1, ...), custom_call_target="tpu_custom_call" | custom-call | tf_op jit(solution)/shard_map/pallas_call | solution.py:747
  146.6 0.0 copy-start.6
  146.7 0.0 copy-start.8
  146.7 8.1 %convolution_bitcast_fusion.2 = f32[1,4096,256]{2,1,0:T(8,128)} fusion(bf16[1024,4096]{1,0:T(8,128)(2,1)} %get-tuple-element.18, bf16[1024,256]{1,0:T(8,128)(2,1)} %get-tuple-element.19), kind=kOutput, calls=%fused_computation.2 | convolution fusion | flops 2147483648 | bytes 13107200 | tf_op jit(solution)/shard_map/dot_general | solution.py:759
  154.7 0.0 copy-done.6
  154.7 0.0 copy-done.8
  154.7 0.0 copy-start.5
  154.7 0.0 copy-start.4
  154.8 4.5 %convolution_bitcast_fusion.1 = f32[1,4096,256]{2,1,0:T(8,128)} fusion(bf16[1024,4096]{1,0:T(8,128)(2,1)S(1)} %copy-done.6, bf16[1024,256]{1,0:T(8,128)(2,1)S(1)} %copy-done.8), kind=kOutput, calls=%fused_computation.1 | convolution fusion | flops 2147483648 | bytes 13107200 | tf_op jit(solution)/shard_map/dot_general | solution.py:759
  159.2 0.0 copy-done.5
  159.3 0.0 collective-permute-done
  159.3 0.0 collective-permute-done.1
  159.3 0.0 copy-done.4
  159.3 0.9 fusion.5.refs_1_
  160.2 23.0 %shard_map.172 = (bf16[256,2048]{1,0:T(8,128)(2,1)}, bf16[4,256,512]{2,1,0:T(8,128)(2,1)}) custom-call(bf16[256,512]{1,0:T(8,128)(2,1)} %get-tuple-element.15.refs_0_, bf16[256,512]{1,0:T(8,128)(2,1)} %fusion.5.refs_1_), custom_call_target="tpu_custom_call" | custom-call | tf_op jit(solution)/shard_map/pallas_call | solution.py:131
  183.2 0.0 copy-start
  183.2 3.1 %shard_map.173 = bf16[256,2048]{1,0:T(8,128)(2,1)} custom-call(bf16[256,2048]{1,0:T(8,128)(2,1)} %get-tuple-element.16.refs_0_), custom_call_target="tpu_custom_call" | custom-call | tf_op jit(solution)/shard_map/pallas_call | solution.py:131
  186.3 0.0 copy-done
  186.3 1.4 broadcast_select_fusion
  187.9 2.5 %copy.23 = bf16[256,4096]{0,1:T(8,128)(2,1)} copy(bf16[256,4096]{1,0:T(8,128)(2,1)S(1)} %slice_dynamic-update-slice_fusion) | data formatting | bytes 4194304 | tf_op jit(solution)/shard_map/all_to_all | solution.py:780
  190.3 4.7 %all-to-all-start = ((bf16[256,4,1024]{0,2,1:T(8,128)(2,1)}), bf16[256,4,1024]{0,2,1:T(8,128)(2,1)}, u32[]{:S(2)}, u32[]{:S(2)}) async-start(bf16[256,4,1024]{0,2,1:T(8,128)(2,1)} %bitcast.6), calls=%async_computation | async-start | bytes 4194304 | tf_op jit(solution)/shard_map/all_to_all | solution.py:780
  195.0 0.0 copy-start.3
  195.1 4.3 %convert_multiply_fusion.3 = (f32[256,512]{1,0:T(8,128)S(1)}, bf16[256,512]{1,0:T(8,128)(2,1)}) fusion(bf16[256,512]{1,0:T(8,128)(2,1)S(1)} %copy-done.4, f32[512]{0:T(512)S(1)} %bitcast.36, f32[1,512]{1,0:T(1,128)S(1)} %collective-permute-done.1, f32[256,512]{1,0:T(8,128)S(1)} %convert_multiply_fusion.1, f32[512]{0:T(512)S(1)} %bitcast.39, ...), kind=kOutput, calls=%fused_computation.11 | convolution fusion | flops 1075183616 | bytes 7874560 | tf_op jit(solution)/shard_map/dot_general | solution.py:771
  199.4 1.3 collective-permute-start.2
  200.7 4.5 %collective-permute-start.3 = (f32[1,512]{1,0:T(1,128)S(1)}, f32[1,512]{1,0:T(1,128)S(1)}, u32[]{:S(2)}, u32[]{:S(2)}) collective-permute-start(f32[1,512]{1,0:T(1,128)S(1)} %get-tuple-element.28), channel_id=1, source_target_pairs={{0,8},{8,16},{16,24},{1,9},{9,17},{17,25},{2,10},{10,18},{18,26},{... | collective-permute-start | bytes 6152 | tf_op jit(solution)/shard_map/ppermute | solution.py:171
  205.2 0.0 copy-done.3
  205.3 0.0 copy-start.1
  205.3 0.0 copy-start.2
  205.3 0.0 copy-start.7
  205.3 7.9 %convolution_bitcast_fusion = f32[1,256,4096]{2,1,0:T(8,128)} fusion(bf16[1024,256]{1,0:T(8,128)(2,1)S(1)} %copy-done.3, bf16[1024,4096]{1,0:T(8,128)(2,1)} %get-tuple-element.22), kind=kOutput, calls=%fused_computation | convolution fusion | flops 2147483648 | bytes 13107200 | tf_op jit(solution)/shard_map/dot_general | solution.py:759
  213.2 7.4 %collective-permute-done.2 = f32[1,512]{1,0:T(1,128)S(1)} collective-permute-done((f32[1,512]{1,0:T(1,128)S(1)}, f32[1,512]{1,0:T(1,128)S(1)}, u32[]{:S(2)}, u32[]{:S(2)}) %collective-permute-start.2) | collective-permute-done | bytes 2080 | tf_op jit(solution)/shard_map/ppermute | solution.py:172
  220.6 0.0 collective-permute-done.3
  220.6 0.0 copy-done.1
  220.6 0.0 copy-done.2
  220.6 1.0 fusion.6
  221.7 0.0 all-to-all-done
  221.7 0.0 copy-done.7
  221.7 4.2 %fusion.2 = f32[1024,512]{1,0:T(8,128)} fusion(bf16[4,256,512]{2,1,0:T(8,128)(2,1)S(1)} %copy-done.7, bf16[256,4,1024]{0,2,1:T(8,128)(2,1)} %all-to-all-done), kind=kOutput, calls=%fused_computation.5 | convolution fusion | flops 1073741824 | bytes 5242880 | tf_op jit(solution)/shard_map/dot_general | solution.py:781
  (11 shorter events, 0.2 us)
Async XLA Ops:
  1.7 157.5 %collective-permute-start = (f32[1,512]{1,0:T(1,128)S(1)}, f32[1,512]{1,0:T(1,128)S(1)}, u32[]{:S(2)}, u32[]{:S(2)}) collective-permute-start(f32[1,512]{1,0:T(1,128)S(1)} %get-tuple-element.31), channel_id=1, source_target_pairs={{0,8},{8,16},{16,24},{1,9},{9,17},{17,25},{2,10},{10,18},{18,26},{... | collective-permute-start | bytes 6152 | tf_op jit(solution)/shard_map/ppermute | solution.py:171
  6.6 152.7 %collective-permute-start.1 = (f32[1,512]{1,0:T(1,128)S(1)}, f32[1,512]{1,0:T(1,128)S(1)}, u32[]{:S(2)}, u32[]{:S(2)}) collective-permute-start(f32[1,512]{1,0:T(1,128)S(1)} %get-tuple-element.32), channel_id=1, source_target_pairs={{8,0},{16,8},{24,16},{9,1},{17,9},{25,17},{10,2},{18,10},{26,18},{... | collective-permute-start | bytes 6152 | tf_op jit(solution)/shard_map/ppermute | solution.py:172
  146.6 8.1 %copy-start.6 = (bf16[1024,4096]{1,0:T(8,128)(2,1)S(1)}, bf16[1024,4096]{1,0:T(8,128)(2,1)}, u32[]{:S(2)}) copy-start(bf16[1024,4096]{1,0:T(8,128)(2,1)} %get-tuple-element.18) | copy-start | bytes 25165828
  146.7 8.1 %copy-start.8 = (bf16[1024,256]{1,0:T(8,128)(2,1)S(1)}, bf16[1024,256]{1,0:T(8,128)(2,1)}, u32[]{:S(2)}) copy-start(bf16[1024,256]{1,0:T(8,128)(2,1)} %get-tuple-element.20) | copy-start | bytes 1572868
  154.7 4.5 %copy-start.5 = (f32[3,512]{1,0:T(4,128)S(1)}, f32[3,512]{1,0:T(4,128)}, u32[]{:S(2)}) copy-start(f32[3,512]{1,0:T(4,128)} %param.16) | copy-start | bytes 18436
  154.7 4.6 %copy-start.4 = (bf16[256,512]{1,0:T(8,128)(2,1)S(1)}, bf16[256,512]{1,0:T(8,128)(2,1)}, u32[]{:S(2)}) copy-start(bf16[256,512]{1,0:T(8,128)(2,1)} %param.13) | copy-start | bytes 786436
  183.2 3.1 %copy-start = (bf16[256,2048]{1,0:T(8,128)(2,1)S(1)}, bf16[256,2048]{1,0:T(8,128)(2,1)}, u32[]{:S(2)}) copy-start(bf16[256,2048]{1,0:T(8,128)(2,1)} %get-tuple-element.16.refs_0_) | copy-start | bytes 3145732
  190.3 31.3 %all-to-all-start = ((bf16[256,4,1024]{0,2,1:T(8,128)(2,1)}), bf16[256,4,1024]{0,2,1:T(8,128)(2,1)}, u32[]{:S(2)}, u32[]{:S(2)}) async-start(bf16[256,4,1024]{0,2,1:T(8,128)(2,1)} %bitcast.6), calls=%async_computation | async-start | bytes 4194304 | tf_op jit(solution)/shard_map/all_to_all | solution.py:780
  195.0 10.2 %copy-start.3 = (bf16[1024,256]{1,0:T(8,128)(2,1)S(1)}, bf16[1024,256]{1,0:T(8,128)(2,1)}, u32[]{:S(2)}) copy-start(bf16[1024,256]{1,0:T(8,128)(2,1)} %get-tuple-element.21) | copy-start | bytes 1572868
  199.4 21.2 %collective-permute-start.2 = (f32[1,512]{1,0:T(1,128)S(1)}, f32[1,512]{1,0:T(1,128)S(1)}, u32[]{:S(2)}, u32[]{:S(2)}) collective-permute-start(f32[1,512]{1,0:T(1,128)S(1)} %get-tuple-element.27), channel_id=1, source_target_pairs={{8,0},{16,8},{24,16},{9,1},{17,9},{25,17},{10,2},{18,10},{26,18},{... | collective-permute-start | bytes 6152 | tf_op jit(solution)/shard_map/ppermute | solution.py:172
  200.7 19.9 %collective-permute-start.3 = (f32[1,512]{1,0:T(1,128)S(1)}, f32[1,512]{1,0:T(1,128)S(1)}, u32[]{:S(2)}, u32[]{:S(2)}) collective-permute-start(f32[1,512]{1,0:T(1,128)S(1)} %get-tuple-element.28), channel_id=1, source_target_pairs={{0,8},{8,16},{16,24},{1,9},{9,17},{17,25},{2,10},{10,18},{18,26},{... | collective-permute-start | bytes 6152 | tf_op jit(solution)/shard_map/ppermute | solution.py:171
  205.3 15.4 %copy-start.1 = (bf16[256,512]{1,0:T(8,128)(2,1)S(1)}, bf16[256,512]{1,0:T(8,128)(2,1)}, u32[]{:S(2)}) copy-start(bf16[256,512]{1,0:T(8,128)(2,1)} %param.15) | copy-start | bytes 786436
  205.3 15.3 %copy-start.2 = (bf16[256,512]{1,0:T(8,128)(2,1)S(1)}, bf16[256,512]{1,0:T(8,128)(2,1)}, u32[]{:S(2)}) copy-start(bf16[256,512]{1,0:T(8,128)(2,1)} %param.14) | copy-start | bytes 786436
  205.3 16.4 %copy-start.7 = (bf16[4,256,512]{2,1,0:T(8,128)(2,1)S(1)}, bf16[4,256,512]{2,1,0:T(8,128)(2,1)}, u32[]{:S(2)}) copy-start(bf16[4,256,512]{2,1,0:T(8,128)(2,1)} %get-tuple-element.17) | copy-start | bytes 3145732

commit v2 on v0

--- a/solution.py
+++ b/solution.py
@@ -324,9 +324,929 @@
     )
 
 
+def flip(index, bits):
+    high, low = (lax.div(index, 2), lax.rem(index, 2))
+    bit_high, bit_low = (lax.div(bits, 2), lax.rem(bits, 2)) if not isinstance(bits, int) else (bits // 2, bits % 2)
+    high = high + bit_high - 2 * high * bit_high
+    low = low + bit_low - 2 * low * bit_low
+    return 2 * high + low
+
+
+def place():
+    sp, tp = (lax.axis_index("sp"), lax.axis_index("tp"))
+    return sp, lax.div(tp, 2), lax.rem(tp, 2)
+
+
+def greet(devices):
+    barrier = pltpu.get_barrier_semaphore()
+    for device in devices:
+        pl.semaphore_signal(barrier, inc=1, device_id=device, device_id_type=MESH)
+    pl.semaphore_wait(barrier, len(devices))
+
+
+def remote(source, target, send_sem, recv_sem, device):
+    return pltpu.make_async_remote_copy(
+        src_ref=source,
+        dst_ref=target,
+        send_sem=send_sem,
+        recv_sem=recv_sem,
+        device_id=device,
+        device_id_type=MESH,
+    )
+
+
+def dot_nt(a, b):
+    return lax.dot_general(a, b, (((1,), (1,)), ((), ())), preferred_element_type=jnp.float32)
+
+
+def dot_nn(a, b):
+    return jnp.dot(a, b, preferred_element_type=jnp.float32)
+
+
+def dot_tn(a, b):
+    return lax.dot_general(a, b, (((0,), (0,)), ((), ())), preferred_element_type=jnp.float32)
+
+
+def experts_kernel(tokens, width, hidden):
+    groups, layers = (4, 4)
+    parts = 2 * layers
+    rows_all = groups * tokens
+
+    def kernel(
+        x_hbm, c_hbm, route, wg_hbm, wu_hbm, wd_hbm, og_hbm, ig_hbm, va_hbm, taps, op_hbm,
+        gg_out, gu_out, gd_out, gog_out, gig_out, gva_out, gop_out,
+        xc, w, wd, wp, acc, acc_down, a, a_far, ht, stage, wrow, sums,
+        sd, sx, sy, sz, rd, rx, ry, rz,
+        op, m, cols_in, mixed, ci, gc, conv, gm, gates, outs_v,
+        load, xc_send, xc_recv, wr_send, wr_recv, wp_send, wp_recv, a_send, a_recv,
+        rs_send, rs_recv, z_send, z_recv, out_sem, st_sem, gd_sem,
+        edge_send, edge_recv, mx_send, mx_recv, m_send, m_recv, a2_send, a2_recv, a2p_send, a2p_recv,
+    ):
+        sp, z, c = place()
+        tp = 2 * z + c
+        xn, yn, dn = (flip(sp, 1), flip(sp, 2), flip(sp, 3))
+        near = 1 - c
+        partner = (sp, 2 * z + near)
+        x_dev, y_dev, d_dev = ((xn, tp), (yn, tp), (dn, tp))
+
+        mid = lax.rem(lax.div(z, 2) + lax.rem(z, 2), 2)
+        inner = mid == 1
+
+        def z_dev(k):
+            return (sp, 2 * flip(z, k) + c)
+
+        def rows(s):
+            return pl.ds(pl.multiple_of(s * tokens, tokens), tokens)
+
+        def blk(t, s, part):
+            return xc.at[t, part, rows(s)]
+
+        loads = [
+            pltpu.make_async_copy(x_hbm, blk(0, sp, tp), load.at[0]),
+            pltpu.make_async_copy(c_hbm, blk(1, sp, tp), load.at[1]),
+            pltpu.make_async_copy(wg_hbm, w.at[:, :, pl.ds(0, hidden)], load.at[2]),
+            pltpu.make_async_copy(wu_hbm, w.at[:, :, pl.ds(hidden, hidden)], load.at[3]),
+            pltpu.make_async_copy(route.at[sp], wrow.at[sp], load.at[4]),
+        ]
+        for part in range(parts):
+            loads.append(
+                pltpu.make_async_copy(
+                    wd_hbm.at[:, pl.ds(part * width, width)], wd.at[part], load.at[5 + part]
+                )
+            )
+        conv_loads = [
+            pltpu.make_async_copy(source, gates.at[j], load.at[5 + parts + j])
+            for j, source in enumerate((og_hbm, ig_hbm, va_hbm))
+        ]
+        op_load = pltpu.make_async_copy(op_hbm, op, load.at[8 + parts])
+        for copy in loads[:2] + conv_loads + loads[2:] + [op_load]:
+            copy.start()
+        pad = 8
+        middle = pl.ds(pad, tokens)
+
+        def edges(buffer, phase):
+            before, after = (lax.rem(sp + groups - 1, groups), lax.rem(sp + 1, groups))
+            top, low = (pl.ds(0, pad), pl.ds(pad + tokens, pad))
+            first, final = (pl.ds(pad, pad), pl.ds(tokens, pad))
+            return [
+                remote(
+                    buffer.at[final], buffer.at[top], edge_send.at[phase, 0], edge_recv.at[phase, 0], (after, tp)
+                ),
+                remote(
+                    buffer.at[first], buffer.at[low], edge_send.at[phase, 1], edge_recv.at[phase, 1], (before, tp)
+                ),
+            ]
+
+        def close_edges(buffer, copies):
+            for copy in copies:
+                copy.wait_recv()
+
+            @pl.when(sp == 0)
+            def _():
+                buffer[pl.ds(0, pad), :] = jnp.zeros((pad, width), jnp.float32)
+
+            @pl.when(sp == groups - 1)
+            def _():
+                buffer[pl.ds(pad + tokens, pad), :] = jnp.zeros((pad, width), jnp.float32)
+
+        ci_edges = edges(ci, 0)
+        greet([partner, z_dev(1), z_dev(2), z_dev(3), x_dev, y_dev, d_dev])
+        loads[0].wait()
+        loads[1].wait()
+
+        def pass_on(t, s, part, slot, device):
+            return remote(
+                blk(t, s, part), blk(t, s, part), xc_send.at[t, slot], xc_recv.at[t, s, part], device
+            )
+
+        def arrive(t, s, part):
+            pass_on(t, s, part, 0, partner).wait_recv()
+
+        for t in (0, 1):
+            pass_on(t, sp, tp, 12, z_dev(1)).start()
+
+            @pl.when(inner)
+            def _():
+                pass_on(t, sp, tp, 13, z_dev(3)).start()
+
+            pass_on(t, sp, tp, 4, x_dev).start()
+            pass_on(t, sp, tp, 8, y_dev).start()
+            pass_on(t, sp, tp, 0, partner).start()
+        for copy in conv_loads:
+            copy.wait()
+        ci[middle, :] = gates[1].astype(jnp.float32) * gates[2].astype(jnp.float32)
+        for copy in ci_edges:
+            copy.start()
+        route_copies = []
+        for i, (s, device) in enumerate(((xn, x_dev), (yn, y_dev), (dn, d_dev))):
+            copy = remote(route.at[s], wrow.at[sp], wr_send.at[i], wr_recv.at[i], device)
+            copy.start()
+            route_copies.append(copy)
+        for copy in loads[2:]:
+            copy.wait()
+        weight_copies = []
+        for part in range(layers):
+            copy = remote(w.at[2 * part + near], wp.at[part], wp_send.at[part], wp_recv.at[part], partner)
+            copy.start()
+            weight_copies.append(copy)
+        acc[...] = jnp.zeros_like(acc)
+        acc_down[...] = jnp.zeros_like(acc_down)
+
+        @pl.when(mid == 0)
+        def _():
+            rz[...] = jnp.zeros_like(rz)
+
+        def multiply(t, layer):
+            @pl.when(t == 0)
+            def _():
+                @pl.loop(0, groups)
+                def _(s):
+                    here = rows(s)
+                    acc[here, :] += dot_nn(xc[0, 2 * layer, here, :], w[2 * layer]) + dot_nn(
+                        xc[0, 2 * layer + 1, here, :], w[2 * layer + 1]
+                    )
+
+            @pl.when(t == 1)
+            def _():
+                @pl.loop(0, groups)
+                def _(s):
+                    here = rows(s)
+                    acc_down[here, :] += dot_nt(xc[1, 2 * layer, here, :], wd[2 * layer]) + dot_nt(
+                        xc[1, 2 * layer + 1, here, :], wd[2 * layer + 1]
+                    )
+
+        def turn(i):
+            return flip(z, i + mid * lax.div(i, 2) * (5 - 2 * i))
+
+        def step(i, carry):
+            r, t = (lax.div(i, 2), lax.rem(i, 2))
+
+            def onward(s, part, m, slot):
+                @pl.when(inner & (m == 1))
+                def _():
+                    pass_on(t, s, part, slot, z_dev(3)).start()
+
+                @pl.when(inner & (m > 1))
+                def _():
+                    pass_on(t, s, part, slot + m - 1, z_dev(1)).start()
+
+            @pl.when(i < 6)
+            def _():
+                part = 2 * turn(r + 1) + c
+                arrive(t, sp, part)
+                onward(sp, part, r + 1, 28)
+                pass_on(t, sp, part, 5 + r, x_dev).start()
+                pass_on(t, sp, part, 9 + r, y_dev).start()
+                pass_on(t, sp, part, 1 + r, partner).start()
+
+            @pl.when(i < 8)
+            def _():
+                part = 2 * turn(r) + c
+                even = lax.rem(r, 2) == 0
+                arrive(t, xn, part)
+
+                @pl.when(even & (t * r == 0))
+                def _():
+                    pass_on(t, xn, part, 31 + r, y_dev).start()
+
+                pass_on(t, xn, part, 15 + r, partner).start()
+                arrive(t, yn, part)
+
+                @pl.when((lax.rem(r, 2) == 1) & (t * r == 0))
+                def _():
+                    pass_on(t, yn, part, 31 + r, x_dev).start()
+
+                pass_on(t, yn, part, 19 + r, partner).start()
+
+            @pl.when((i >= 2) & (i < 10))
+            def _():
+                m = r - 1
+                part = 2 * turn(m) + c
+                arrive(t, dn, part)
+
+                @pl.when((t == 1) & (m == 0))
+                def _():
+                    pass_on(t, dn, part, 35, z_dev(1)).start()
+
+                    @pl.when(inner)
+                    def _():
+                        pass_on(t, dn, part, 36, z_dev(3)).start()
+
+                @pl.when((t == 1) & (m > 0))
+                def _():
+                    onward(dn, part, m, 37)
+
+                pass_on(t, dn, part, 22 + r, partner).start()
+
+            @pl.when(i == 2)
+            def _():
+                close_edges(ci, ci_edges)
+                conv[...] = (
+                    ci[pl.ds(pad - 1, tokens), :] * taps[0:1, :]
+                    + ci[middle, :] * taps[1:2, :]
+                    + ci[pl.ds(pad + 1, tokens), :] * taps[2:3, :]
+                )
+                mixed[sp] = (gates[0].astype(jnp.float32) * conv[...]).astype(jnp.bfloat16)
+
+            @pl.when(i >= 3)
+            def _():
+                j = i - 3
+                kj, tj = (lax.div(j, 2), lax.rem(j, 2))
+                layer = turn(kj)
+                for s in range(groups):
+                    arrive(tj, s, 2 * layer + near)
+                multiply(tj, layer)
+
+            return carry
+
+        lax.fori_loop(0, 11, step, 0)
+
+        for copy in route_copies:
+            copy.wait()
+        for copy in weight_copies:
+            copy.wait()
+        half = 128
+        eye = lax.broadcasted_iota(jnp.int32, (half, half), 0) == lax.broadcasted_iota(
+            jnp.int32, (half, half), 1
+        )
+        a_copies = []
+
+        def gate_rows(i, s):
+            columns = []
+            for h in range(tokens // half):
+                line = jnp.broadcast_to(wrow[s, 0:1, h * half : (h + 1) * half], (half, half))
+                columns.append(jnp.sum(jnp.where(eye, line, 0.0), axis=1, keepdims=True))
+
+            for h in range(tokens // half):
+                start = pl.multiple_of(s * tokens + h * half, half)
+                here = pl.ds(start, half)
+                gate, up = (acc[here, pl.ds(0, hidden)], acc[here, pl.ds(hidden, hidden)])
+                back = acc_down[here, :] * columns[h]
+                sig = jax.nn.sigmoid(gate)
+                act = gate * sig
+                a[here, pl.ds(0, hidden)] = (back * up * sig * (1.0 + gate * (1.0 - sig))).astype(jnp.bfloat16)
+                a[here, pl.ds(hidden, hidden)] = (back * act).astype(jnp.bfloat16)
+                ht[:, pl.ds(start, half)] = (act * up * columns[h]).T.astype(jnp.bfloat16)
+            copy = remote(a.at[rows(s)], a_far.at[rows(s)], a_send.at[i], a_recv.at[i], partner)
+            copy.start()
+            a_copies.append(copy)
+
+        def weight_copy(j, slot, part):
+            target = (gg_out, gu_out)[j]
+            return pltpu.make_async_copy(stage.at[slot, j], target.at[part], st_sem.at[slot, j])
+
+        def down_copy(part):
+            cols = pl.ds(pl.multiple_of(part * width, width), width)
+            return pltpu.make_async_copy(wd.at[part], gd_out.at[:, cols], gd_sem.at[part])
+
+        def weight_grads(first, stop):
+            tile = 256
+
+            @pl.loop(first, stop)
+            def _(part):
+                slot = lax.rem(part, 2)
+
+                @pl.when(part >= 2)
+                def _():
+                    for j in (0, 1):
+                        weight_copy(j, slot, part).wait()
+
+                @pl.loop(0, width // tile)
+                def _(n):
+                    feats = pl.ds(pl.multiple_of(n * tile, tile), tile)
+                    totals = [0.0, 0.0]
+                    for g in range(groups):
+                        here = pl.ds(g * tokens, tokens)
+                        turned = xc[0, part, here, feats].T
+                        for j in (0, 1):
+                            totals[j] += dot_nn(turned, a[here, pl.ds(j * hidden, hidden)])
+                    for j in (0, 1):
+                        stage[slot, j, feats, :] = totals[j].astype(jnp.bfloat16)
+
+                    wd[part, :, feats] = dot_nn(ht[...], xc[1, part, :, feats]).astype(jnp.bfloat16)
+
+                for j in (0, 1):
+                    weight_copy(j, slot, part).start()
+                down_copy(part).start()
+
+        chunks = 4
+        span = tokens // chunks
+
+        def part_rows(q):
+            return pl.ds(pl.multiple_of(q * span, span), span)
+
+        def partial(s, k, finish):
+            layer = flip(z, k)
+            value = dot_nt(a[rows(s), :], w[2 * layer + c]) + dot_nt(a_far[rows(s), :], wp[layer])
+            finish[k] = value.astype(finish.dtype)
+
+        def rs_copy(kind, k, q, device):
+            source, target = ((sd, rd), (sx, rx), (sy, ry))[kind]
+            return remote(
+                source.at[k, part_rows(q)],
+                target.at[k, part_rows(q)],
+                rs_send.at[kind, k, q],
+                rs_recv.at[kind, k, q],
+                device,
+            )
+
+        def landed(kind, k, q):
+            rs_copy(kind, k, q, partner).wait_recv()
+
+        def wide(ref):
+            return ref.astype(jnp.float32)
+
+        def merge(kind, k, q):
+            landed(0, k, q)
+            here = part_rows(q)
+            buffer = (None, sx, sy)[kind]
+            buffer[k, here, :] = (wide(buffer[k, here, :]) + wide(rd[k, here, :])).astype(jnp.bfloat16)
+            rs_copy(kind, k, q, (None, x_dev, y_dev)[kind]).start()
+
+        def stage_a(q):
+            rs_copy(0, 2, q, x_dev).start()
+            rs_copy(0, 3, q, y_dev).start()
+            rs_copy(1, 2, q, x_dev).start()
+            rs_copy(2, 3, q, y_dev).start()
+            rs_copy(0, 0, q, x_dev).start()
+            rs_copy(0, 1, q, y_dev).start()
+
+        def stage_b(q):
+            merge(2, 2, q)
+            merge(1, 3, q)
+            rs_copy(1, 0, q, x_dev).start()
+            rs_copy(2, 1, q, y_dev).start()
+
+        def stage_c(q):
+            merge(2, 0, q)
+            merge(1, 1, q)
+
+        def z_ship(k, q):
+            to = flip(z, 1) if k == 1 else flip(z, 1 + 2 * mid)
+            slot = {1: 0, 2: 3 + 2 * mid, 3: 2 + 2 * mid}[k]
+            return remote(
+                sz.at[k, part_rows(q)],
+                rz.at[slot, part_rows(q)],
+                z_send.at[k, q],
+                z_recv.at[slot, q],
+                (sp, 2 * to + c),
+            )
+
+        def z_landed(slot, q):
+            remote(
+                sz.at[0, part_rows(q)], rz.at[slot, part_rows(q)], z_send.at[0, q], z_recv.at[slot, q], partner
+            ).wait_recv()
+
+        def collect(k, q):
+            landed(1, k, q)
+            landed(2, k, q)
+            here = part_rows(q)
+            total = sums[k, here, :] + wide(rx[k, here, :]) + wide(ry[k, here, :])
+            sums[k, here, :] = total
+            if k:
+
+                @pl.when(mid == 0)
+                def _():
+                    sz[k, here, :] = total.astype(jnp.bfloat16)
+                    z_ship(k, q).start()
+
+        def pass_along(k, q):
+            here = part_rows(q)
+            slot = {1: 5, 2: 2, 3: 3}[k]
+
+            @pl.when(inner)
+            def _():
+                z_landed(slot, q)
+                total = sums[k, here, :] + wide(rz[slot, here, :])
+                sz[k, here, :] = total.astype(jnp.bfloat16)
+                z_ship(k, q).start()
+
+        def m_copy(q, part, slot, device):
+            return remote(
+                m.at[part, part_rows(q)],
+                m.at[part, part_rows(q)],
+                m_send.at[q, slot],
+                m_recv.at[q, part],
+                device,
+            )
+
+        def conclude(q):
+            here = part_rows(q)
+            z_landed(0, q)
+
+            @pl.when(inner)
+            def _():
+                z_landed(4, q)
+
+            mine = pl.ds(pl.multiple_of(sp * tokens + q * span, span), span)
+            total = sums[0, here, :] + wide(xc[1, tp, mine, :])
+            total += wide(rz[0, here, :]) + wide(rz[4, here, :])
+            m[tp, here, :] = total.astype(jnp.bfloat16)
+            for k in (3, 2, 1):
+                m_copy(q, tp, k, z_dev(k)).start()
+            m_copy(q, tp, 0, partner).start()
+
+        def across(q, k):
+            layer = flip(z, k)
+            return layer != sp, remote(
+                m.at[2 * layer + c, part_rows(q)],
+                cols_in.at[sp, c, part_rows(q)],
+                a2_send.at[q, k],
+                a2_recv.at[q, sp],
+                (layer, tp),
+            )
+
+        def beside(q, s, side):
+            return remote(
+                cols_in.at[s, side, part_rows(q)],
+                cols_in.at[s, side, part_rows(q)],
+                a2p_send.at[q, s],
+                a2p_recv.at[q, s],
+                partner,
+            )
+
+        def spread(q):
+            for k in (0, 3, 2, 1):
+                part = 2 * flip(z, k) + c
+                if k:
+                    m_copy(q, part, 0, partner).wait_recv()
+                    m_copy(q, part, 3 + k, partner).start()
+                needed, copy = across(q, k)
+
+                @pl.when(needed)
+                def _():
+                    copy.start()
+
+        def project(q):
+            here = part_rows(q)
+            for layer in range(layers):
+                m_copy(q, 2 * layer + near, 0, partner).wait_recv()
+            total = dot_nn(m[0, here, :], op[0])
+            for part in range(1, parts):
+                total += dot_nn(m[part, here, :], op[part])
+            gm[here, :] = total
+
+        def relay(q):
+            for d in (1, 2, 3):
+                s = lax.rem(sp + d, groups)
+                remote(
+                    m.at[tp, part_rows(q)], cols_in.at[s, c, part_rows(q)], a2_send.at[q, 0], a2_recv.at[q, s], partner
+                ).wait_recv()
+                beside(q, s, c).start()
+
+        def partner_rows(i):
+            a_copies[i].wait_recv()
+
+        gate_rows(0, dn)
+        gate_rows(1, xn)
+        partner_rows(0)
+        partial(dn, 2, sd)
+        rs_copy(0, 2, 0, x_dev).start()
+        partial(dn, 3, sd)
+        rs_copy(0, 3, 0, y_dev).start()
+        gate_rows(2, yn)
+        partner_rows(1)
+        partial(xn, 2, sx)
+        rs_copy(1, 2, 0, x_dev).start()
+        gate_rows(3, sp)
+        partner_rows(2)
+        partial(yn, 3, sy)
+        rs_copy(2, 3, 0, y_dev).start()
+        partial(dn, 0, sd)
+        rs_copy(0, 0, 0, x_dev).start()
+        partial(dn, 1, sd)
+        rs_copy(0, 1, 0, y_dev).start()
+        stage_a(1)
+        partner_rows(3)
+        partial(yn, 2, sy)
+        partial(xn, 3, sx)
+        partial(xn, 0, sx)
+        partial(yn, 1, sy)
+        mixed_copies = [
+            remote(mixed.at[sp], mixed.at[sp], mx_send.at[i], mx_recv.at[sp], device)
+            for i, device in enumerate((x_dev, y_dev, d_dev))
+        ]
+
+        def during(q, first, last, work):
+            @pl.when((q >= first) & (q <= last))
+            def _():
+                work(q - first)
+
+        def round_trip(q, carry):
+            @pl.when(q == 0)
+            def _():
+                stage_b(0)
+                partial(yn, 0, sy)
+                partial(xn, 1, sx)
+                stage_c(0)
+                stage_a(2)
+                for k in (3, 2, 1, 0):
+                    partial(sp, k, sums)
+
+            def ends(i):
+                collect(1, i)
+                collect(0, i)
+
+            during(q, 1, chunks, ends)
+            during(q, 2, chunks + 1, conclude)
+            during(q, 3, chunks + 2, spread)
+            during(q, 1, chunks - 1, lambda i: stage_b(i + 1))
+
+            def handed(i):
+                pass_along(2, i)
+                pass_along(3, i)
+
+            during(q, 1, chunks, handed)
+            during(q, 0, chunks - 1, lambda i: weight_grads(2 * i, 2 * i + 1))
+            during(q, 1, chunks - 1, lambda i: stage_c(i + 1))
+
+            @pl.when(q == 1)
+            def _():
+                stage_a(3)
+
+
+            @pl.when(q == chunks - 1)
+            def _():
+                for copy in mixed_copies:
+                    copy.start()
+
+            def middle_collect(i):
+                collect(3, i)
+                collect(2, i)
+
+            during(q, 0, chunks - 1, middle_collect)
+            during(q, 1, chunks, lambda i: pass_along(1, i))
+            during(q, 0, chunks - 1, lambda i: weight_grads(2 * i + 1, 2 * i + 2))
+            during(q, 4, chunks + 3, project)
+            during(q, 4, chunks + 3, relay)
+            return carry
+
+        op_load.wait()
+        lax.fori_loop(0, chunks + 4, round_trip, 0)
+        gc[middle, :] = gm[...] * gates[0].astype(jnp.float32)
+        gc_edges = edges(gc, 1)
+        for copy in gc_edges:
+            copy.start()
+        outs_v[0] = (gm[...] * conv[...]).astype(jnp.bfloat16)
+        finals = [pltpu.make_async_copy(outs_v.at[0], gog_out, out_sem.at[3])]
+        finals[0].start()
+        for s in (xn, yn, dn):
+            remote(mixed.at[s], mixed.at[s], mx_send.at[0], mx_recv.at[s], partner).wait_recv()
+
+        @pl.loop(0, chunks)
+        def _(q):
+            for d in (1, 2, 3):
+                beside(q, lax.rem(sp + d, groups), near).wait_recv()
+
+
+        tile = width // 2
+
+        @pl.loop(0, 2)
+        def _(side):
+            @pl.loop(0, 2)
+            def _(n):
+                feats = pl.ds(pl.multiple_of(n * tile, tile), tile)
+                total = dot_nn(m[2 * sp + side, :, feats].T, mixed[sp])
+                for d in (1, 2, 3):
+                    s = lax.rem(sp + d, groups)
+                    total += dot_nn(cols_in[s, side, :, feats].T, mixed[s])
+                acc[pl.ds(pl.multiple_of(side * width + n * tile, tile), tile), :] = total
+
+        copy = pltpu.make_async_copy(acc, gop_out, out_sem.at[4])
+        copy.start()
+        finals.append(copy)
+        close_edges(gc, gc_edges)
+        grad = (
+            gc[pl.ds(pad + 1, tokens), :] * taps[0:1, :]
+            + gc[middle, :] * taps[1:2, :]
+            + gc[pl.ds(pad - 1, tokens), :] * taps[2:3, :]
+        )
+        outs_v[1] = (grad * gates[2].astype(jnp.float32)).astype(jnp.bfloat16)
+        outs_v[2] = (grad * gates[1].astype(jnp.float32)).astype(jnp.bfloat16)
+        for j, target in ((1, gig_out), (2, gva_out)):
+            copy = pltpu.make_async_copy(outs_v.at[j], target, out_sem.at[5 + j])
+            copy.start()
+            finals.append(copy)
+        for copy in a_copies + mixed_copies + ci_edges + gc_edges:
+            copy.wait_send()
+
+        @pl.loop(0, chunks)
+        def _(q):
+            for kind, ks in ((0, range(4)), (1, range(4)), (2, range(4))):
+                for k in ks:
+                    rs_copy(kind, k, q, partner).wait_send()
+            for slot in range(7):
+                m_copy(q, tp, slot, partner).wait_send()
+            for k in (1, 2, 3):
+                z_ship(k, q).wait_send()
+            for k in range(4):
+                needed, copy = across(q, k)
+
+                @pl.when(needed)
+                def _():
+                    copy.wait_send()
+
+            for d in (1, 2, 3):
+                beside(q, lax.rem(sp + d, groups), c).wait_send()
+
+        for t in (0, 1):
+
+            def sent(slot):
+                pass_on(t, sp, tp, slot, partner).wait_send()
+
+            pl.loop(0, 13)(sent)
+            pl.loop(15, 27)(sent)
+            if t:
+                sent(31)
+                sent(35)
+            else:
+                pl.loop(31, 35)(sent)
+
+            @pl.when(inner)
+            def _():
+                sent(13)
+                pl.loop(28, 31)(sent)
+                if t:
+                    pl.loop(36, 40)(sent)
+
+        for slot in (0, 1):
+            for j in (0, 1):
+                weight_copy(j, slot, slot).wait()
+        for part in range(parts):
+            down_copy(part).wait()
+        for copy in finals:
+            copy.wait()
+
+    block_shape = (layers, tokens, width)
+    shapes = [
+        jax.ShapeDtypeStruct((parts, width, hidden), jnp.bfloat16),
+        jax.ShapeDtypeStruct((parts, width, hidden), jnp.bfloat16),
+        jax.ShapeDtypeStruct((hidden, parts * width), jnp.bfloat16),
+    ]
+    shapes += [jax.ShapeDtypeStruct((tokens, width), jnp.bfloat16)] * 3
+    shapes.append(jax.ShapeDtypeStruct((2 * width, width), jnp.float32))
+    half = jnp.bfloat16
+    return pl.pallas_call(
+        kernel,
+        out_shape=shapes,
+        in_specs=[pl.BlockSpec(memory_space=pl.ANY)] * 9
+        + [pl.BlockSpec(memory_space=pltpu.VMEM), pl.BlockSpec(memory_space=pl.ANY)],
+        out_specs=[pl.BlockSpec(memory_space=pl.ANY)] * 7,
+        scratch_shapes=[
+            pltpu.VMEM((2, parts, rows_all, width), half),
+            pltpu.VMEM((parts, width, 2 * hidden), half),
+            pltpu.VMEM((parts, hidden, width), half),
+            pltpu.VMEM((layers, width, 2 * hidden), half),
+            pltpu.VMEM((rows_all, 2 * hidden), jnp.float32),
+            pltpu.VMEM((rows_all, hidden), jnp.float32),
+            pltpu.VMEM((rows_all, 2 * hidden), half),
+            pltpu.VMEM((rows_all, 2 * hidden), half),
+            pltpu.VMEM((hidden, rows_all), half),
+            pltpu.VMEM((2, 2, width, hidden), half),
+            pltpu.VMEM((groups, 8, tokens), jnp.float32),
+            pltpu.VMEM(block_shape, jnp.float32),
+        ]
+        + [pltpu.VMEM(block_shape, half)] * 7
+        + [
+            pltpu.VMEM((6, tokens, width), half),
+            pltpu.VMEM((parts, width, width), half),
+            pltpu.VMEM((parts, tokens, width), half),
+            pltpu.VMEM((groups, 2, tokens, width), half),
+            pltpu.VMEM((groups, tokens, width), half),
+            pltpu.VMEM((tokens + 16, width), jnp.float32),
+            pltpu.VMEM((tokens + 16, width), jnp.float32),
+            pltpu.VMEM((tokens, width), jnp.float32),
+            pltpu.VMEM((tokens, width), jnp.float32),
+            pltpu.VMEM((3, tokens, width), half),
+            pltpu.VMEM((3, tokens, width), half),
+            pltpu.SemaphoreType.DMA((9 + parts,)),
+            pltpu.SemaphoreType.DMA((2, 40)),
+            pltpu.SemaphoreType.DMA((2, groups, parts)),
+            pltpu.SemaphoreType.DMA((3,)),
+            pltpu.SemaphoreType.DMA((3,)),
+            pltpu.SemaphoreType.DMA((layers,)),
+            pltpu.SemaphoreType.DMA((layers,)),
+            pltpu.SemaphoreType.DMA((groups,)),
+            pltpu.SemaphoreType.DMA((groups,)),
+            pltpu.SemaphoreType.DMA((3, layers, 4)),
+            pltpu.SemaphoreType.DMA((3, layers, 4)),
+            pltpu.SemaphoreType.DMA((layers, 4)),
+            pltpu.SemaphoreType.DMA((6, 4)),
+            pltpu.SemaphoreType.DMA((8,)),
+            pltpu.SemaphoreType.DMA((2, 2)),
+            pltpu.SemaphoreType.DMA((parts,)),
+            pltpu.SemaphoreType.DMA((2, 2)),
+            pltpu.SemaphoreType.DMA((2, 2)),
+            pltpu.SemaphoreType.DMA((3,)),
+            pltpu.SemaphoreType.DMA((groups,)),
+            pltpu.SemaphoreType.DMA((4, 7)),
+            pltpu.SemaphoreType.DMA((4, parts)),
+            pltpu.SemaphoreType.DMA((4, layers)),
+            pltpu.SemaphoreType.DMA((4, groups)),
+            pltpu.SemaphoreType.DMA((4, groups)),
+            pltpu.SemaphoreType.DMA((4, groups)),
+        ],
+        compiler_params=pltpu.CompilerParams(
+            collective_id=10, has_side_effects=True, vmem_limit_bytes=62 * 1024 * 1024
+        ),
+    )
+
+
+def finish(grads, rest):
+    pieces = 4
+    count, total = (len(grads), len(grads) + len(rest))
+
+    def kernel(*refs):
+        sources, targets = (refs[:total], refs[total : 2 * total])
+        narrow, broad = (refs[2 * total : 2 * total + count], refs[2 * total + count : 2 * total + 2 * count])
+        through = refs[2 * total + 2 * count : 3 * total + count]
+        in_sem, out_sem = refs[-2:]
+
+        def piece(ref, i):
+            size = ref.shape[0] // pieces
+            return ref.at[pl.ds(i * size, size)]
+
+        fetches = {}
+        for i in range(pieces):
+            for j in range(count):
+                fetches[i, j] = pltpu.make_async_copy(
+                    piece(sources[j], i), piece(narrow[j], i), in_sem.at[j, i]
+                )
+                fetches[i, j].start()
+        for j in range(count, total):
+            fetches[0, j] = pltpu.make_async_copy(sources[j], through[j - count], in_sem.at[j, 0])
+            fetches[0, j].start()
+        stores = []
+
+        def store(source, target, j, i):
+            copy = pltpu.make_async_copy(source, target, out_sem.at[j, i])
+            copy.start()
+            stores.append(copy)
+
+        for i in range(pieces):
+            for j in range(count):
+                fetches[i, j].wait()
+                size = narrow[j].shape[0] // pieces
+                steps = 4
+                rows = size // steps
+
+                @pl.loop(0, steps)
+                def _(n):
+                    here = pl.ds(pl.multiple_of(i * size + n * rows, rows), rows)
+                    broad[j][here, :] = narrow[j][here, :].astype(jnp.float32)
+
+                store(piece(broad[j], i), piece(targets[j], i), j, i)
+        for j in range(count, total):
+            fetches[0, j].wait()
+            store(through[j - count], targets[j], j, 0)
+        for copy in stores:
+            copy.wait()
+
+    shapes = [jax.ShapeDtypeStruct(g.shape, jnp.float32) for g in grads]
+    shapes += [jax.ShapeDtypeStruct(r.shape, r.dtype) for r in rest]
+    return pl.pallas_call(
+        kernel,
+        out_shape=shapes,
+        in_specs=[pl.BlockSpec(memory_space=pl.ANY)] * total,
+        out_specs=[pl.BlockSpec(memory_space=pl.ANY)] * total,
+        scratch_shapes=[pltpu.VMEM(g.shape, g.dtype) for g in grads]
+        + [pltpu.VMEM(g.shape, jnp.float32) for g in grads]
+        + [pltpu.VMEM(r.shape, r.dtype) for r in rest]
+        + [pltpu.SemaphoreType.DMA((total, pieces))] * 2,
+        compiler_params=pltpu.CompilerParams(vmem_limit_bytes=62 * 1024 * 1024),
+    )(*grads, *rest)
+
+
+def near_body(
+    moe_input,
+    out_gate,
+    in_gate,
+    values,
+    conv_taps,
+    out_proj,
+    route_ids,
+    route_gates,
+    expert_gate,
+    expert_up,
+    expert_down,
+    cotangent,
+):
+    token_count, part_width = moe_input.shape
+    group_count = lax.axis_size("sp")
+    hidden = expert_gate.shape[2]
+    part_count = lax.axis_size("tp")
+    chosen = route_ids[None, :, :] == jnp.arange(group_count, dtype=jnp.int32)[:, None, None]
+    weights = jnp.sum(jnp.where(chosen, route_gates[None, :, :], 0.0), axis=2)
+    route = jnp.broadcast_to(weights[:, None, :], (group_count, 8, token_count))
+    (
+        grad_expert_gate,
+        grad_expert_up,
+        grad_expert_down,
+        grad_out_gate,
+        grad_in_gate,
+        grad_values,
+        grad_out_proj,
+    ) = experts_kernel(token_count, part_width, hidden)(
+        moe_input,
+        cotangent,
+        route,
+        expert_gate.reshape(part_count, part_width, hidden),
+        expert_up.reshape(part_count, part_width, hidden),
+        expert_down[0],
+        out_gate,
+        in_gate,
+        values,
+        conv_taps,
+        out_proj.reshape(part_count, part_width, part_width),
+    )
+
+    (
+        grad_expert_gate,
+        grad_expert_up,
+        grad_expert_down,
+        grad_out_gate,
+        grad_in_gate,
+        grad_values,
+        grad_out_proj,
+    ) = finish(
+        (
+            grad_expert_gate.reshape(-1, hidden),
+            grad_expert_up.reshape(-1, hidden),
+            grad_expert_down,
+        ),
+        (grad_out_gate, grad_in_gate, grad_values, grad_out_proj),
+    )
+    grad_expert_gate = grad_expert_gate[None]
+    grad_expert_up = grad_expert_up[None]
+    grad_expert_down = grad_expert_down[None]
+    return (
+        grad_out_gate,
+        grad_in_gate,
+        grad_values,
+        grad_out_proj,
+        grad_expert_gate,
+        grad_expert_up,
+        grad_expert_down,
+    )
+
+
+def step(*arrays):
+    moe_input, expert_gate, out_proj = (arrays[0], arrays[8], arrays[5])
+    tokens, width = moe_input.shape
+    near = (
+        lax.axis_size("sp") == 4
+        and lax.axis_size("tp") == 8
+        and expert_gate.shape[0] == 1
+        and tokens % 256 == 0
+        and width == 2 * expert_gate.shape[2] == 2 * tokens
+        and out_proj.shape[0] == 8 * width
+    )
+    return (near_body if near else body)(*arrays)
+
+
 def solution(mesh):
     return jax.shard_map(
-        body,
+        step,
         mesh=mesh,
         in_specs=(
             P("sp", "tp"),

time: 317 us -> 171 us (0.54)
  matrix products: 49.9 us -> 0 us
  Pallas kernels: 202 us -> 169 us
  other arithmetic: 21.5 us -> 0.71 us
  local copies, waits for them, and re-layouts: 18.8 us -> 0.62 us
  starting transfers between devices: 16.9 us -> 0 us
  waiting for transfers between devices: 3.72 us -> 0 us
    dot_general x14 -> x0, matrix products: 49.9 us -> none  [the longest x1 6.68 us: body(): jnp.einsum('prf,prd->pfd', hidden_act, full_cot, preferred_element_type=j...]
    pallas_call x9 -> x2, Pallas kernels: 202 us -> 169 us  [the longest x1 160 us: near_body(): experts_kernel(token_count, part_width, hidden)]
    ppermute x4 -> x0, starting transfers between devices: 12.3 us -> none  [the longest x2 9.68 us: padded(): before = lax.ppermute(last, axis, up)]
    unnamed x68 -> x0, local copies, waits for them, and re-layouts: 9.91 us -> none
    convert_element_type x6 -> x0, other arithmetic: 7.63 us -> none  [the longest x1 2.16 us: body(): chip_rows = (halves(partial_rows, part_width).astype(jnp.float32) + other...]
    select_n x2 -> x0, other arithmetic: 6.93 us -> none  [interleave(): jnp.where(core == 0, other, own)]
    all_to_all x1 -> x0, starting transfers between devices: 4.63 us -> none  [body(): lax.all_to_all(full_mixer_cot, 'sp', split_axis=1, concat_axis=0, tiled=T...]
    all_to_all x1 -> x0, local copies, waits for them, and re-layouts: 4.08 us -> none  [body(): lax.all_to_all(full_mixer_cot, 'sp', split_axis=1, concat_axis=0, tiled=T...]
  transfers between devices with their start and end apart: 5 -> 0, of which waited for: 1 -> 0; matrix products, arithmetic and copies ran while one was open for 8% -> 0% of each run, Pallas kernels for 0% -> 0%
where the time goes in v2:
time: 171 us
  Pallas kernels  169 us (99%)
    pallas_call x1, Pallas kernels, near_body(): experts_kernel(token_count, part_width, hidden)  160 us
    pallas_call x1, Pallas kernels, finish(): pl.pallas_call(kernel, out_shape=shapes, in_specs=[pl.BlockSpec(memory_sp...  9.29 us

profile of v2, /device:TPU:0, one launch (start us, length us, event | category | flops | bytes accessed | tf_op | source)
XLA Modules:
  0.0 170.9 jit_solution(8642809499989074711)
XLA Ops:
  0.6 0.7 select_reduce_fusion
  1.3 0.6 broadcast_in_dim.32.route
  2.0 159.6 %shard_map.171 = (bf16[8,512,256]{2,1,0:T(8,128)(2,1)}, bf16[8,512,256]{2,1,0:T(8,128)(2,1)}, bf16[256,4096]{1,0:T(8,128)(2,1)}, bf16[256,512]{1,0:T(8,128)(2,1)...) custom-call(bf16[256,512]{1,0:T(8,128)(2,1)} %x_hbm.1, bf16[256,512]{1,0:T(8,128)(2,1)} %c_hbm.1, ...), custom_call_target="tpu_custom_call" | custom-call | tf_op jit(solution)/shard_map/pallas_call | solution.py:1189
  161.6 9.3 %shard_map.172 = (f32[4096,256]{1,0:T(8,128)}, f32[4096,256]{1,0:T(8,128)}, f32[256,4096]{1,0:T(8,128)}, bf16[256,512]{1,0:T(8,128)(2,1)}, bf16[256,512]{1,0:T(8...) custom-call(bf16[4096,256]{1,0:T(8,128)(2,1)} %bitcast.13, bf16[4096,256]{1,0:T(8,128)(2,1)} %bitcast.14, ...), custom_call_target="tpu_custom_call" | custom-call | tf_op jit(solution)/shard_map/pallas_call | solution.py:1147

commit v3 on v2

--- a/solution.py
+++ b/solution.py
@@ -459,6 +459,11 @@
                 blk(t, s, part), blk(t, s, part), xc_send.at[t, slot], xc_recv.at[t, s, part], device
             )
 
+        def pass_half(s, part, h, slot, device):
+            here = pl.ds(pl.multiple_of(s * tokens + h * (tokens // 2), tokens // 2), tokens // 2)
+            block = xc.at[1, part, here]
+            return remote(block, block, xc_send.at[1, slot], xc_recv.at[1, s, part], device)
+
         def arrive(t, s, part):
             pass_on(t, s, part, 0, partner).wait_recv()
 
@@ -545,16 +550,24 @@
                 even = lax.rem(r, 2) == 0
                 arrive(t, xn, part)
 
-                @pl.when(even & (t * r == 0))
+                @pl.when(even & (t == 0))
                 def _():
                     pass_on(t, xn, part, 31 + r, y_dev).start()
 
+                @pl.when((r == 0) & (t == 1))
+                def _():
+                    pass_half(xn, part, 0, 31, y_dev).start()
+
                 pass_on(t, xn, part, 15 + r, partner).start()
                 arrive(t, yn, part)
 
-                @pl.when((lax.rem(r, 2) == 1) & (t * r == 0))
+                @pl.when((lax.rem(r, 2) == 1) & (t == 0))
                 def _():
                     pass_on(t, yn, part, 31 + r, x_dev).start()
+
+                @pl.when((r == 0) & (t == 1))
+                def _():
+                    pass_half(yn, part, 1, 32, x_dev).start()
 
                 pass_on(t, yn, part, 19 + r, partner).start()
 
@@ -722,8 +735,10 @@
             merge(1, 1, q)
 
         def z_ship(k, q):
-            to = flip(z, 1) if k == 1 else flip(z, 1 + 2 * mid)
-            slot = {1: 0, 2: 3 + 2 * mid, 3: 2 + 2 * mid}[k]
+            straight = lax.div(q, chunks - 1)
+            hop = 1 if k == 1 else (1 + 2 * mid) * (1 - straight) + k * straight
+            to = flip(z, hop)
+            slot = {1: 0, 2: 3 + 2 * mid, 3: 2 + 2 * mid}[k] * (1 - straight) + k * straight
             return remote(
                 sz.at[k, part_rows(q)],
                 rz.at[slot, part_rows(q)],
@@ -745,7 +760,7 @@
             sums[k, here, :] = total
             if k:
 
-                @pl.when(mid == 0)
+                @pl.when((mid == 0) | (q == chunks - 1))
                 def _():
                     sz[k, here, :] = total.astype(jnp.bfloat16)
                     z_ship(k, q).start()
@@ -772,16 +787,28 @@
 
         def conclude(q):
             here = part_rows(q)
-            z_landed(0, q)
-
-            @pl.when(inner)
-            def _():
-                z_landed(4, q)
-
             mine = pl.ds(pl.multiple_of(sp * tokens + q * span, span), span)
-            total = sums[0, here, :] + wide(xc[1, tp, mine, :])
-            total += wide(rz[0, here, :]) + wide(rz[4, here, :])
-            m[tp, here, :] = total.astype(jnp.bfloat16)
+
+            @pl.when(q < chunks - 1)
+            def _():
+                z_landed(0, q)
+
+                @pl.when(inner)
+                def _():
+                    z_landed(4, q)
+
+                total = sums[0, here, :] + wide(xc[1, tp, mine, :])
+                total += wide(rz[0, here, :]) + wide(rz[4, here, :])
+                m[tp, here, :] = total.astype(jnp.bfloat16)
+
+            @pl.when(q == chunks - 1)
+            def _():
+                total = sums[0, here, :] + wide(xc[1, tp, mine, :])
+                for k in (1, 2, 3):
+                    z_landed(k, q)
+                    total += wide(rz[k, here, :])
+                m[tp, here, :] = total.astype(jnp.bfloat16)
+
             for k in (3, 2, 1):
                 m_copy(q, tp, k, z_dev(k)).start()
             m_copy(q, tp, 0, partner).start()
@@ -872,57 +899,60 @@
             def _():
                 work(q - first)
 
-        def round_trip(q, carry):
-            @pl.when(q == 0)
-            def _():
-                stage_b(0)
-                partial(yn, 0, sy)
-                partial(xn, 1, sx)
-                stage_c(0)
-                stage_a(2)
-                for k in (3, 2, 1, 0):
-                    partial(sp, k, sums)
-
-            def ends(i):
-                collect(1, i)
-                collect(0, i)
-
-            during(q, 1, chunks, ends)
-            during(q, 2, chunks + 1, conclude)
-            during(q, 3, chunks + 2, spread)
-            during(q, 1, chunks - 1, lambda i: stage_b(i + 1))
-
-            def handed(i):
-                pass_along(2, i)
-                pass_along(3, i)
-
-            during(q, 1, chunks, handed)
-            during(q, 0, chunks - 1, lambda i: weight_grads(2 * i, 2 * i + 1))
-            during(q, 1, chunks - 1, lambda i: stage_c(i + 1))
-
-            @pl.when(q == 1)
-            def _():
-                stage_a(3)
-
-
-            @pl.when(q == chunks - 1)
+        last = chunks - 1
+        stage_b(0)
+        partial(yn, 0, sy)
+        partial(xn, 1, sx)
+        stage_c(0)
+        stage_a(2)
+        for k in (3, 2, 1, 0):
+            partial(sp, k, sums)
+
+        def merge_next(i):
+            stage_b(i + 1)
+            stage_c(i + 1)
+
+            @pl.when(i + 3 <= last)
+            def _():
+                stage_a(i + 3)
+
+            @pl.when(i + 1 == last)
             def _():
                 for copy in mixed_copies:
                     copy.start()
 
-            def middle_collect(i):
-                collect(3, i)
-                collect(2, i)
-
-            during(q, 0, chunks - 1, middle_collect)
-            during(q, 1, chunks, lambda i: pass_along(1, i))
-            during(q, 0, chunks - 1, lambda i: weight_grads(2 * i + 1, 2 * i + 2))
-            during(q, 4, chunks + 3, project)
-            during(q, 4, chunks + 3, relay)
+        def far_collect(i):
+            collect(3, i)
+            collect(2, i)
+
+        def near_collect(i):
+            collect(1, i)
+            collect(0, i)
+
+        def handed(i):
+            pass_along(2, i)
+            pass_along(3, i)
+
+        def spare(i):
+            project(i)
+            relay(i)
+
+        def round_trip(q, carry):
+            during(q, 1, chunks - 1, lambda i: pass_along(1, i))
+            during(q, 0, last - 1, merge_next)
+            during(q, 0, last, lambda i: weight_grads(2 * i, 2 * i + 1))
+            during(q, 0, last, far_collect)
+            during(q, 1, chunks, conclude)
+            during(q, 2, chunks + 1, spread)
+            during(q, 0, last, near_collect)
+            during(q, 0, last - 1, handed)
+            during(q, 0, last, lambda i: weight_grads(2 * i + 1, 2 * i + 2))
+            during(q, 3, chunks + 1, spare)
             return carry
 
         op_load.wait()
-        lax.fori_loop(0, chunks + 4, round_trip, 0)
+        lax.fori_loop(0, chunks + 2, round_trip, 0)
+        project(last)
         gc[middle, :] = gm[...] * gates[0].astype(jnp.float32)
         gc_edges = edges(gc, 1)
         for copy in gc_edges:
@@ -930,19 +960,27 @@
         outs_v[0] = (gm[...] * conv[...]).astype(jnp.bfloat16)
         finals = [pltpu.make_async_copy(outs_v.at[0], gog_out, out_sem.at[3])]
         finals[0].start()
+        relay(last)
         for s in (xn, yn, dn):
             remote(mixed.at[s], mixed.at[s], mx_send.at[0], mx_recv.at[s], partner).wait_recv()
 
-        @pl.loop(0, chunks)
-        def _(q):
-            for d in (1, 2, 3):
-                beside(q, lax.rem(sp + d, groups), near).wait_recv()
-
-
         tile = width // 2
 
+        def out_side(side):
+            here = pl.ds(pl.multiple_of(side * width, width), width)
+            return pltpu.make_async_copy(acc.at[here], gop_out.at[here], out_sem.at[4 + side])
+
         @pl.loop(0, 2)
-        def _(side):
+        def _(turn_of):
+            side = lax.rem(c + turn_of, 2)
+
+            @pl.when(turn_of == 1)
+            def _():
+                @pl.loop(0, chunks)
+                def _(q):
+                    for d in (1, 2, 3):
+                        beside(q, lax.rem(sp + d, groups), near).wait_recv()
+
             @pl.loop(0, 2)
             def _(n):
                 feats = pl.ds(pl.multiple_of(n * tile, tile), tile)
@@ -952,9 +990,9 @@
                     total += dot_nn(cols_in[s, side, :, feats].T, mixed[s])
                 acc[pl.ds(pl.multiple_of(side * width + n * tile, tile), tile), :] = total
 
-        copy = pltpu.make_async_copy(acc, gop_out, out_sem.at[4])
-        copy.start()
-        finals.append(copy)
+            out_side(side).start()
+
+        finals += [out_side(0), out_side(1)]
         close_edges(gc, gc_edges)
         grad = (
             gc[pl.ds(pad + 1, tokens), :] * taps[0:1, :]
@@ -997,7 +1035,8 @@
             pl.loop(0, 13)(sent)
             pl.loop(15, 27)(sent)
             if t:
-                sent(31)
+                pass_half(sp, tp, 0, 31, partner).wait_send()
+                pass_half(sp, tp, 0, 32, partner).wait_send()
                 sent(35)
             else:
                 pl.loop(31, 35)(sent)
@@ -1175,9 +1214,12 @@
     group_count = lax.axis_size("sp")
     hidden = expert_gate.shape[2]
     part_count = lax.axis_size("tp")
-    chosen = route_ids[None, :, :] == jnp.arange(group_count, dtype=jnp.int32)[:, None, None]
-    weights = jnp.sum(jnp.where(chosen, route_gates[None, :, :], 0.0), axis=2)
-    route = jnp.broadcast_to(weights[:, None, :], (group_count, 8, token_count))
+    shape = (group_count, 8, token_count)
+    expert = lax.broadcasted_iota(jnp.int32, shape, 0)
+    route = jnp.zeros(shape, jnp.float32)
+    for pick in range(route_ids.shape[1]):
+        chosen = route_ids[:, pick][None, None, :] == expert
+        route += jnp.where(chosen, route_gates[:, pick][None, None, :], 0.0)
     (
         grad_expert_gate,
         grad_expert_up,

time: 171 us -> 167 us (0.977)
  Pallas kernels: 169 us -> 164 us
    pallas_call x1, Pallas kernels: 160 us -> 154 us  [near_body(): experts_kernel(token_count, part_width, hidden)]
where the time goes in v3:
time: 167 us; the launch traced here: 166 us
  Pallas kernels  164 us (98%)
    pallas_call x1, Pallas kernels, near_body(): experts_kernel(token_count, part_width, hidden)  154 us
    pallas_call x1, Pallas kernels, finish(): pl.pallas_call(kernel, out_shape=shapes, in_specs=[pl.BlockSpec(memory_sp...  9.29 us

profile of v3, /device:TPU:0, one launch (start us, length us, event | category | flops | bytes accessed | tf_op | source)
XLA Modules:
  0.0 166.5 jit_solution(12499781523904633016)
XLA Ops:
  0.6 0.8 fusion
  1.4 0.8 fusion.1
  2.2 0.6 select_add_fusion.route
  2.8 154.4 %shard_map.171 = (bf16[8,512,256]{2,1,0:T(8,128)(2,1)}, bf16[8,512,256]{2,1,0:T(8,128)(2,1)}, bf16[256,4096]{1,0:T(8,128)(2,1)}, bf16[256,512]{1,0:T(8,128)(2,1)...) custom-call(bf16[256,512]{1,0:T(8,128)(2,1)} %x_hbm.1, bf16[256,512]{1,0:T(8,128)(2,1)} %c_hbm.1, ...), custom_call_target="tpu_custom_call" | custom-call | tf_op jit(solution)/shard_map/pallas_call | solution.py:1231
  157.2 9.3 %shard_map.172 = (f32[4096,256]{1,0:T(8,128)}, f32[4096,256]{1,0:T(8,128)}, f32[256,4096]{1,0:T(8,128)}, bf16[256,512]{1,0:T(8,128)(2,1)}, bf16[256,512]{1,0:T(8...) custom-call(bf16[4096,256]{1,0:T(8,128)(2,1)} %bitcast.17, bf16[4096,256]{1,0:T(8,128)(2,1)} %bitcast.18, ...), custom_call_target="tpu_custom_call" | custom-call | tf_op jit(solution)/shard_map/pallas_call | solution.py:1186

commit v4 on v3

--- a/solution.py
+++ b/solution.py
@@ -419,7 +419,7 @@
             for j, source in enumerate((og_hbm, ig_hbm, va_hbm))
         ]
         op_load = pltpu.make_async_copy(op_hbm, op, load.at[8 + parts])
-        for copy in loads[:2] + conv_loads + loads[2:] + [op_load]:
+        for copy in loads[:2]:
             copy.start()
         pad = 8
         middle = pl.ds(pad, tokens)
@@ -477,6 +477,8 @@
             pass_on(t, sp, tp, 4, x_dev).start()
             pass_on(t, sp, tp, 8, y_dev).start()
             pass_on(t, sp, tp, 0, partner).start()
+        for copy in conv_loads + loads[2:] + [op_load]:
+            copy.start()
         for copy in conv_loads:
             copy.wait()
         ci[middle, :] = gates[1].astype(jnp.float32) * gates[2].astype(jnp.float32)
@@ -1214,12 +1216,9 @@
     group_count = lax.axis_size("sp")
     hidden = expert_gate.shape[2]
     part_count = lax.axis_size("tp")
-    shape = (group_count, 8, token_count)
-    expert = lax.broadcasted_iota(jnp.int32, shape, 0)
-    route = jnp.zeros(shape, jnp.float32)
-    for pick in range(route_ids.shape[1]):
-        chosen = route_ids[:, pick][None, None, :] == expert
-        route += jnp.where(chosen, route_gates[:, pick][None, None, :], 0.0)
+    chosen = route_ids[None, :, :] == jnp.arange(group_count, dtype=jnp.int32)[:, None, None]
+    weights = jnp.sum(jnp.where(chosen, route_gates[None, :, :], 0.0), axis=2)
+    route = jnp.broadcast_to(weights[:, None, :], (group_count, 8, token_count))
     (
         grad_expert_gate,
         grad_expert_up,

time: 167 us -> 166 us (level)
  no operation moved by 1% of the time
where the time goes in v4:
time: 166 us
  Pallas kernels  164 us (99%)
    pallas_call x1, Pallas kernels, near_body(): experts_kernel(token_count, part_width, hidden)  155 us
    pallas_call x1, Pallas kernels, finish(): pl.pallas_call(kernel, out_shape=shapes, in_specs=[pl.BlockSpec(memory_sp...  9.29 us

profile of v4, /device:TPU:0, one launch (start us, length us, event | category | flops | bytes accessed | tf_op | source)
XLA Modules:
  0.0 166.0 jit_solution(3841696203522389908)
XLA Ops:
  0.6 0.7 select_reduce_fusion
  1.3 0.6 broadcast_in_dim.32.route
  2.0 154.7 %shard_map.171 = (bf16[8,512,256]{2,1,0:T(8,128)(2,1)}, bf16[8,512,256]{2,1,0:T(8,128)(2,1)}, bf16[256,4096]{1,0:T(8,128)(2,1)}, bf16[256,512]{1,0:T(8,128)(2,1)...) custom-call(bf16[256,512]{1,0:T(8,128)(2,1)} %x_hbm.1, bf16[256,512]{1,0:T(8,128)(2,1)} %c_hbm.1, ...), custom_call_target="tpu_custom_call" | custom-call | tf_op jit(solution)/shard_map/pallas_call | solution.py:1230
  156.7 9.3 %shard_map.172 = (f32[4096,256]{1,0:T(8,128)}, f32[4096,256]{1,0:T(8,128)}, f32[256,4096]{1,0:T(8,128)}, bf16[256,512]{1,0:T(8,128)(2,1)}, bf16[256,512]{1,0:T(8...) custom-call(bf16[4096,256]{1,0:T(8,128)(2,1)} %bitcast.13, bf16[4096,256]{1,0:T(8,128)(2,1)} %bitcast.14, ...), custom_call_target="tpu_custom_call" | custom-call | tf_op jit(solution)/shard_map/pallas_call | solution.py:1188
